TPU v7x, 32 devices: a whole 2x2x4 slice. The times are simulated.
32 devices in a mesh: sp: 8 (over z, x), tp: 4 (over y, core).
Axes of the slice: x: 2, y: 2, z: 4, core: 2. Of those that a mesh axis runs over, the one named last changes fastest.
Arguments:
- glu_a: bfloat16 [2048, 1024], P('sp', 'tp'), may hold values from -6 to 6
- glu_b: bfloat16 [2048, 1024], P('sp', 'tp'), may hold values from -6 to 6
- saved_conv: bfloat16 [2048, 1024], P('sp', 'tp')
- taps: float32 [31, 1024], P(None, 'tp'), may hold values from -1 to 1
- norm_gain_vector: float32 [1024], P('tp'), may hold values from 0.1 to 1.9
- out_proj: bfloat16 [1024, 2048], P('tp'), may hold values from -0.1875 to 0.1875
- moe_in: bfloat16 [2048, 2048], P('sp'), may hold values from -6 to 6
- grad_out: bfloat16 [2048, 2048], P('sp'), may hold values from -6 to 6
- expert_ids: int32 [2048, 2], P('sp'), may hold values from 0 to 7, all different within a row; in each aligned block of 256 rows (0 to 255, 256 to 511, ...) at most 96 rows name the same one
- route_weights: float32 [2048, 2], P('sp'), may hold values from 0.3 to 2
- w_gate: bfloat16 [8, 2048, 1024], P('sp', None, 'tp'), may hold values from -0.125 to 0.125
- w_up: bfloat16 [8, 2048, 1024], P('sp', None, 'tp'), may hold values from -0.125 to 0.125
- w_down: bfloat16 [8, 1024, 2048], P('sp', 'tp'), may hold values from -0.1875 to 0.1875
Outputs:
- grad_glu_a: bfloat16 [2048, 1024], P('sp', 'tp')
- grad_glu_b: bfloat16 [2048, 1024], P('sp', 'tp')
- grad_out_proj: float32 [2048, 1024], P('sp', 'tp')
- grad_gate: bfloat16 [8, 2048, 1024], P('sp', None, 'tp')
- grad_up: bfloat16 [8, 2048, 1024], P('sp', None, 'tp')
- grad_down: bfloat16 [8, 1024, 2048], P('sp', 'tp')
Inputs may be any that keep to these rules, and one draw needn't show every extreme that they name: `expert_ids`: in each aligned block of 256 tokens, a token's 2 experts differ, and no expert is named more than 96 times; some expert reaches 96 in some blocks.
All inputs are finite; a program needn't handle non-finite values.
Results may differ from a plain program's by a relative error of at most 0.015.
Values may be sent and summed in bfloat16 or wider, within the bound.
A program may use at most 64 MiB of HBM per device.

v0:
```python
import jax
import jax.numpy as jnp
from jax import lax
from jax.sharding import PartitionSpec as P

CONV_CHANNELS = 1024


def with_halo(array, sides, width):
    for axis, dim in sides:
        size, length = (lax.axis_size(axis), array.shape[dim])
        up = [(i, (i + 1) % size) for i in range(size - 1)]
        down = [(j, i) for i, j in up]
        last = lax.slice_in_dim(array, length - width, length, axis=dim)
        initial = lax.slice_in_dim(array, 0, width, axis=dim)
        before = lax.ppermute(last, axis, up)
        after = lax.ppermute(initial, axis, down)
        array = jnp.concatenate([before, array, after], axis=dim)
    return array


def expert_local(in_rows, cot_rows, w_gate, w_up, w_down):
    gate_pre = jnp.einsum("esd,edf->esf", in_rows, w_gate, preferred_element_type=jnp.float32)
    up_pre = jnp.einsum("esd,edf->esf", in_rows, w_up, preferred_element_type=jnp.float32)
    sig_gate = jax.nn.sigmoid(gate_pre)
    act_gate = gate_pre * sig_gate
    hidden = (act_gate * up_pre).astype(jnp.bfloat16)
    grad_hidden = jnp.einsum("esd,efd->esf", cot_rows, w_down, preferred_element_type=jnp.float32)
    grad_upact = (grad_hidden * act_gate).astype(jnp.bfloat16)
    grad_gateact = (grad_hidden * up_pre * sig_gate * (1.0 + gate_pre * (1.0 - sig_gate))).astype(
        jnp.bfloat16
    )
    return (hidden, grad_upact, grad_gateact)


def weight_grads(in_rows, cot_rows, hidden, grad_upact, grad_gateact):
    grad_down = jnp.einsum(
        "esf,esd->efd", hidden, cot_rows, preferred_element_type=jnp.float32
    ).astype(jnp.bfloat16)
    grad_gate = jnp.einsum(
        "esd,esf->edf", in_rows, grad_gateact, preferred_element_type=jnp.float32
    ).astype(jnp.bfloat16)
    grad_up = jnp.einsum(
        "esd,esf->edf", in_rows, grad_upact, preferred_element_type=jnp.float32
    ).astype(jnp.bfloat16)
    return (grad_gate, grad_up, grad_down)


def per_device(
    glu_a,
    glu_b,
    saved_conv,
    taps,
    norm_gain_vector,
    out_proj,
    moe_in,
    grad_out,
    expert_ids,
    route_weights,
    w_gate,
    w_up,
    w_down,
):
    n_sp = lax.axis_size("sp")
    n_tp = lax.axis_size("tp")
    tp_pos = lax.axis_index("tp")
    tok_dev, d_model = grad_out.shape
    top_count = expert_ids.shape[1]
    exp_dev = w_gate.shape[0]
    experts = exp_dev * n_sp
    capacity = max(2, 3 * tok_dev * top_count // (2 * experts))
    quarter = d_model // n_tp
    pair_count = tok_dev * top_count
    flat_ids = expert_ids.reshape(pair_count)
    onehot = (flat_ids[:, None] == jnp.arange(experts, dtype=jnp.int32)[None, :]).astype(jnp.int32)
    slot_rank = jnp.sum((jnp.cumsum(onehot, axis=0) - onehot) * onehot, axis=1)
    slot_of = flat_ids * capacity + slot_rank
    owner_idx = (
        jnp.full((experts * capacity,), pair_count, jnp.int32)
        .at[slot_of]
        .set(jnp.arange(pair_count, dtype=jnp.int32))
    )
    token_idx = owner_idx // top_count
    scaled = (grad_out.astype(jnp.float32)[:, None, :] * route_weights[:, :, None]).astype(
        jnp.bfloat16
    )
    scaled = scaled.reshape(pair_count, d_model)

    def to_expert(rows):
        width = rows.shape[1]
        return (
            rows.reshape(n_sp, exp_dev, capacity, width)
            .swapaxes(0, 1)
            .reshape(exp_dev, n_sp * capacity, width)
        )

    in_part = lax.dynamic_slice_in_dim(moe_in, tp_pos * quarter, quarter, 1)
    cot_part = lax.dynamic_slice_in_dim(scaled, tp_pos * quarter, quarter, 1)
    in_pad = jnp.concatenate([in_part, jnp.zeros((1, quarter), jnp.bfloat16)], axis=0)
    cot_pad = jnp.concatenate([cot_part, jnp.zeros((1, quarter), jnp.bfloat16)], axis=0)
    sent_in, sent_cot = (
        lax.all_to_all(in_pad[token_idx], "sp", split_axis=0, concat_axis=0, tiled=True),
        lax.all_to_all(cot_pad[owner_idx], "sp", split_axis=0, concat_axis=0, tiled=True),
    )
    recv_in, recv_cot = (
        lax.all_gather(sent_in, "tp", axis=1, tiled=True),
        lax.all_gather(sent_cot, "tp", axis=1, tiled=True),
    )
    in_rows = to_expert(recv_in)
    cot_rows = to_expert(recv_cot)
    hidden, grad_upact, grad_gateact = expert_local(in_rows, cot_rows, w_gate, w_up, w_down)
    grad_gate, grad_up, grad_down = weight_grads(
        in_rows, cot_rows, hidden, grad_upact, grad_gateact
    )
    partial_value = jnp.einsum(
        "esf,edf->esd", grad_gateact, w_gate, preferred_element_type=jnp.float32
    )
    partial_value = partial_value + jnp.einsum(
        "esf,edf->esd", grad_upact, w_up, preferred_element_type=jnp.float32
    )
    partial_value = partial_value.astype(jnp.bfloat16)
    row_grads = (
        lax.psum_scatter(partial_value, "tp", scatter_dimension=2, tiled=True)
        .astype(jnp.float32)
        .astype(jnp.bfloat16)
    )
    row_grads = (
        row_grads.reshape(exp_dev, n_sp, capacity, quarter)
        .swapaxes(0, 1)
        .reshape(n_sp * exp_dev * capacity, quarter)
    )
    returned = lax.all_to_all(row_grads, "sp", split_axis=0, concat_axis=0, tiled=True)
    picked = returned[slot_of].reshape(tok_dev, top_count, quarter).astype(jnp.float32)
    grad_own = lax.dynamic_slice_in_dim(grad_out, tp_pos * quarter, quarter, 1).astype(jnp.float32)
    mix_part = (grad_own + jnp.sum(picked, axis=1)).astype(jnp.bfloat16)
    grad_mix = lax.all_gather(mix_part, "tp", axis=1, tiled=True)
    head_gradient = lax.dot_general(
        grad_mix, out_proj, (((1,), (1,)), ((), ())), preferred_element_type=jnp.float32
    )
    convolved_rows = saved_conv.astype(jnp.float32)
    sum_c, sum_sq = lax.psum(
        (jnp.sum(convolved_rows, axis=1), jnp.sum(convolved_rows * convolved_rows, axis=1)), "tp"
    )
    channel_average = (sum_c / CONV_CHANNELS)[:, None]
    var_c = (sum_sq / CONV_CHANNELS)[:, None] - channel_average * channel_average
    inverse_deviation = lax.rsqrt(var_c + 1e-05)
    centered_scaled = (convolved_rows - channel_average) * inverse_deviation
    normalized_rows = centered_scaled * norm_gain_vector[None, :]
    sigmoid_of_norm = jax.nn.sigmoid(normalized_rows)
    heads = (normalized_rows * sigmoid_of_norm).astype(jnp.bfloat16)
    grad_out_proj = lax.psum_scatter(
        lax.dot_general(
            grad_mix, heads, (((0,), (0,)), ((), ())), preferred_element_type=jnp.float32
        ),
        "sp",
        scatter_dimension=0,
        tiled=True,
    )
    normalized_gradient = (
        head_gradient
        * sigmoid_of_norm
        * (1.0 + normalized_rows * (1.0 - sigmoid_of_norm))
        * norm_gain_vector[None, :]
    )
    gradient_total, product_total = lax.psum(
        (
            jnp.sum(normalized_gradient, axis=1),
            jnp.sum(normalized_gradient * centered_scaled, axis=1),
        ),
        "tp",
    )
    convolved_gradient = (
        inverse_deviation
        * (
            normalized_gradient
            - (gradient_total / CONV_CHANNELS)[:, None]
            - centered_scaled * (product_total / CONV_CHANNELS)[:, None]
        )
    ).astype(jnp.bfloat16)
    reach = (taps.shape[0] - 1) // 2
    padded = with_halo(convolved_gradient, (("sp", 0),), reach).astype(jnp.float32)
    grad_y = jnp.zeros(head_gradient.shape, jnp.float32)
    for tap_idx in range(taps.shape[0]):
        grad_y = (
            grad_y
            + taps[tap_idx][None, :] * padded[2 * reach - tap_idx : 2 * reach - tap_idx + tok_dev]
        )
    sig_b = jax.nn.sigmoid(glu_b.astype(jnp.float32))
    grad_glu_a = (grad_y * sig_b).astype(jnp.bfloat16)
    grad_glu_b = (grad_y * glu_a.astype(jnp.float32) * sig_b * (1.0 - sig_b)).astype(jnp.bfloat16)
    return (grad_glu_a, grad_glu_b, grad_out_proj, grad_gate, grad_up, grad_down)


def solution(mesh):
    in_specs = (
        P("sp", "tp"),
        P("sp", "tp"),
        P("sp", "tp"),
        P(None, "tp"),
        P("tp"),
        P("tp", None),
        P("sp", None),
        P("sp", None),
        P("sp", None),
        P("sp", None),
        P("sp", None, "tp"),
        P("sp", None, "tp"),
        P("sp", "tp", None),
    )
    out_specs = (
        P("sp", "tp"),
        P("sp", "tp"),
        P("sp", "tp"),
        P("sp", None, "tp"),
        P("sp", None, "tp"),
        P("sp", "tp", None),
    )
    return jax.shard_map(
        per_device, mesh=mesh, in_specs=in_specs, out_specs=out_specs, check_vma=False
    )
```

profile of v0, /device:TPU:0, one launch (start us, length us, event | category | flops | bytes accessed | tf_op | source)
XLA Modules:
  0.0 280.5 jit_solution(9579719425612122031)
XLA Ops:
  9.4 1.1 reduce-window.6
  10.9 2.4 scatter_custom_fusion
  14.4 2.7 gather_fusion.1
  17.1 27.3 %all_to_all.36 = bf16[8,96,512]{2,1,0:T(8,128)(2,1)} all-to-all(bf16[8,96,512]{2,1,0:T(8,128)(2,1)S(1)} %bitcast.85), channel_id=1, replica_groups=mesh['sp'=8,'tp'=4] {'sp'}, dimensions={0} | all-to-all | bytes 1572864 | tf_op jit(solution)/shard_map/all_to_all | solution.py:102
  44.8 4.1 %mul.456 = f32[256,2,2048]{2,1,0:T(2,128)} broadcast(bf16[256,2048]{1,0:T(8,128)(2,1)S(1)} %copy-done.1), dimensions={0,2} | broadcast | bytes 5242880 | tf_op jit(solution)/shard_map/mul | solution.py:84
  48.9 6.4 %mul.457 = f32[512,2048]{1,0:T(8,128)} reshape(f32[256,2,2048]{2,1,0:T(2,128)} %mul.456) | data formatting | bytes 8388608 | tf_op jit(solution)/shard_map/mul | solution.py:84
  55.3 1.4 fusion.6
  56.7 2.7 gather_fusion
  59.4 23.1 %all_to_all.37 = bf16[8,96,512]{2,1,0:T(8,128)(2,1)} all-to-all(bf16[8,96,512]{2,1,0:T(8,128)(2,1)S(1)} %bitcast.86), channel_id=1, replica_groups=mesh['sp'=8,'tp'=4] {'sp'}, dimensions={0} | all-to-all | bytes 1572864 | tf_op jit(solution)/shard_map/all_to_all | solution.py:103
  82.7 3.9 %fusion.9 = f32[768,256]{1,0:T(8,128)} fusion(bf16[768,2048]{1,0:T(8,128)(2,1)} %all-gather.6.cloned.1.call-done, bf16[1,2048,256]{2,1,0:T(8,128)(2,1)S(1)} %copy-done), kind=kOutput, calls=%fused_computation.19 | convolution fusion | flops 805306368 | bytes 4980736 | tf_op jit(solution)/shard_map/esd,edf->esf/dot_general | solution.py:23
  86.6 1.9 fusion.12
  88.5 21.8 %all-gather.4.cloned.1.call-done = bf16[768,2048]{1,0:T(8,128)(2,1)} async-done(((bf16[768,512]{1,0:T(8,128)(2,1)}), bf16[768,2048]{1,0:T(8,128)(2,1)}) %all-gather.4.cloned.1.call-update) | async-done | bytes 3145744 | tf_op jit(solution)/shard_map/all_gather | solution.py:107
  110.3 3.8 %multiply_convert_fusion.1 = (bf16[768,256]{1,0:T(8,128)(2,1)S(1)}, bf16[768,256]{1,0:T(8,128)(2,1)S(1)}) fusion(f32[768,256]{1,0:T(8,128)} %fusion.9, f32[768,256]{1,0:T(8,128)} %fusion.12, bf16[768,2048]{1,0:T(8,128)(2,1)} %all-gather.4.cloned.1.call-done, bf16[1,256,2048]{2,1,0:T(8,128)(2,1)} %param.25), kind=kOutput, calls=%fused_computation.27 | convolution fusion | flops 807862272 | bytes 6553600 | tf_op jit(solution)/shard_map/esd,efd->esf/dot_general | solution.py:28
  114.1 1.0 fusion.7
  115.1 2.7 fusion
  117.9 37.9 %reduce-scatter.3.cloned.1.call-done = bf16[1,768,512]{2,1,0:T(8,128)(2,1)} async-done(((bf16[1,768,2048]{2,1,0:T(8,128)(2,1)}), bf16[1,768,512]{2,1,0:T(8,128)(2,1)}) %reduce-scatter.3.cloned.1.call-update) | async-done | bytes 786448 | tf_op jit(solution)/shard_map/reduce_scatter | solution.py:123
  155.8 5.5 %all-to-all-start.2 = ((bf16[8,96,512]{2,1,0:T(8,128)(2,1)}), bf16[8,96,512]{2,1,0:T(8,128)(2,1)S(1)}, u32[]{:S(2)}, u32[]{:S(2)}) async-start(bf16[8,96,512]{2,1,0:T(8,128)(2,1)} %bitcast.89), calls=%async_computation.3 | async-start | bytes 1572864 | tf_op jit(solution)/shard_map/all_to_all | solution.py:132
  161.5 19.8 %all-to-all-done.2 = bf16[8,96,512]{2,1,0:T(8,128)(2,1)S(1)} async-done(((bf16[8,96,512]{2,1,0:T(8,128)(2,1)}), bf16[8,96,512]{2,1,0:T(8,128)(2,1)S(1)}, u32[]{:S(2)}, u32[]{:S(2)}) %all-to-all-start.2) | async-done | bytes 786464 | tf_op jit(solution)/shard_map/all_to_all | solution.py:132
  181.4 2.0 gather_fusion.2
  184.0 1.2 reduce_sum.60
  185.3 1.7 add_convert_fusion.1
  187.2 5.9 %all-reduce.3 = (f32[256]{0:T(256)S(1)}, f32[256]{0:T(256)S(1)}) all-reduce(f32[256]{0:T(256)S(1)} %get-tuple-element.9, f32[256]{0:T(256)S(1)} %get-tuple-element.8), channel_id=1, replica_groups=mesh['sp'=8,'tp'=4] {'tp'}, use_global_device_ids=true, to_apply=%region_3.4 | all-reduce | flops 512 | bytes 4096 | tf_op jit(solution)/shard_map/psum | solution.py:141
  193.2 8.7 %all-gather.8.cloned.1.call-done = bf16[256,2048]{1,0:T(8,128)(2,1)} async-done(((bf16[256,512]{1,0:T(8,128)(2,1)}), bf16[256,2048]{1,0:T(8,128)(2,1)}) %all-gather.8.cloned.1.call-update) | async-done | bytes 1048592 | tf_op jit(solution)/shard_map/all_gather | solution.py:136
  201.9 3.2 %fusion.65 = f32[2048,256]{1,0:T(8,128)} fusion(bf16[256,2048]{1,0:T(8,128)(2,1)} %all-gather.8.cloned.1.call-done, bf16[256,256]{1,0:T(8,128)(2,1)S(1)} %copy-done.2, f32[256]{0:T(256)S(1)} %copy-done.9, f32[256]{0:T(256)S(1)} %get-tuple-element.54, f32[256]{0:T(256)S(1)} %get-tuple-element.53), kind=kOutput, calls=%fused_computation.117 | convolution fusion | flops 269025280 | bytes 3279872 | tf_op jit(solution)/shard_map/dot_general | solution.py:152
  205.1 4.0 %fusion.2 = bf16[1,2048,256]{2,1,0:T(8,128)(2,1)} fusion(bf16[768,2048]{1,0:T(8,128)(2,1)} %all-gather.6.cloned.1.call-done, bf16[768,256]{1,0:T(8,128)(2,1)S(1)} %get-tuple-element.16), kind=kOutput, calls=%fused_computation.10 | convolution fusion | flops 805830656 | bytes 4587520 | tf_op jit(solution)/shard_map/esd,esf->edf/dot_general | solution.py:43
  209.2 2.0 fusion.3
  211.8 6.3 %all-reduce.2 = (f32[256]{0:T(256)S(1)}, f32[256]{0:T(256)S(1)}) all-reduce(f32[256]{0:T(256)S(1)} %get-tuple-element.7, f32[256]{0:T(256)S(1)} %get-tuple-element.6), channel_id=1, replica_groups=mesh['sp'=8,'tp'=4] {'tp'}, use_global_device_ids=true, to_apply=%region_13.14 | all-reduce | flops 512 | bytes 4096 | tf_op jit(solution)/shard_map/psum | solution.py:165
  218.4 3.5 %collective-permute-start = (bf16[15,256]{1,0:T(8,128)(2,1)S(1)}, bf16[15,256]{1,0:T(8,128)(2,1)S(1)}, u32[]{:S(2)}, u32[]{:S(2)}) collective-permute-start(bf16[15,256]{1,0:T(8,128)(2,1)S(1)} %get-tuple-element.18), channel_id=1, source_target_pairs={{0,4},{4,8},{8,12},{12,16},{16,20},{20,24},{24,28},{1,5},{5,9},{9,... | collective-permute-start | bytes 23048 | tf_op jit(solution)/shard_map/ppermute | solution.py:16
  221.9 1.4 collective-permute-start.1
  223.4 3.9 %fusion.1 = bf16[1,2048,256]{2,1,0:T(8,128)(2,1)} fusion(bf16[768,2048]{1,0:T(8,128)(2,1)} %all-gather.6.cloned.1.call-done, bf16[768,256]{1,0:T(8,128)(2,1)S(1)} %get-tuple-element.17), kind=kOutput, calls=%fused_computation.9 | convolution fusion | flops 805830656 | bytes 4587520 | tf_op jit(solution)/shard_map/esd,esf->edf/dot_general | solution.py:40
  227.7 1.6 multiply_convert_fusion.4
  230.0 44.0 %reduce-scatter.5.cloned.1.call-done = f32[256,256]{1,0:T(8,128)} async-done(((f32[2048,256]{1,0:T(8,128)}), f32[256,256]{1,0:T(8,128)}) %reduce-scatter.5.cloned.1.call-update) | async-done | bytes 262160 | tf_op jit(solution)/shard_map/reduce_scatter | solution.py:151
  (76 shorter events, 7.2 us)
Async XLA Ops:
  7.2 75.5 %copy-start = (bf16[1,2048,256]{2,1,0:T(8,128)(2,1)S(1)}, bf16[1,2048,256]{2,1,0:T(8,128)(2,1)}, u32[]{:S(2)}) copy-start(bf16[1,2048,256]{2,1,0:T(8,128)(2,1)} %param.23) | copy-start | bytes 3145732
  7.2 75.5 %all-gather.6.cloned.1.call-start = ((), (), s32[]{:S(2)}) async-start(), calls=%async_computation.6 | async-start | bytes 3932160 | tf_op jit(solution)/shard_map/all_gather | solution.py:106
  14.4 30.1 %copy-start.8 = (f32[256,2]{0,1:T(2,128)S(1)}, f32[256,2]{0,1:T(2,128)}, u32[]{:S(2)}) copy-start(f32[256,2]{0,1:T(2,128)} %param.22) | copy-start | bytes 6148
  14.4 30.4 %copy-start.1 = (bf16[256,2048]{1,0:T(8,128)(2,1)S(1)}, bf16[256,2048]{1,0:T(8,128)(2,1)}, u32[]{:S(2)}) copy-start(bf16[256,2048]{1,0:T(8,128)(2,1)} %param.20) | copy-start | bytes 3145732
  44.5 65.8 %all-gather.4.cloned.1.call-start = ((), (), s32[]{:S(2)}) async-start(), calls=%async_computation.5 | async-start | bytes 3932160 | tf_op jit(solution)/shard_map/all_gather | solution.py:107
  82.6 4.0 %copy-start.4 = (bf16[1,2048,256]{2,1,0:T(8,128)(2,1)S(1)}, bf16[1,2048,256]{2,1,0:T(8,128)(2,1)}, u32[]{:S(2)}) copy-start(bf16[1,2048,256]{2,1,0:T(8,128)(2,1)} %param.24) | copy-start | bytes 3145732
  82.6 73.1 %reduce-scatter.3.cloned.1.call-start = ((), (), s32[]{:S(2)}) async-start(), calls=%async_computation.7 | async-start | bytes 3932160 | tf_op jit(solution)/shard_map/reduce_scatter | solution.py:123
  82.7 3.9 %copy-start.10 = (bf16[768,2048]{1,0:T(8,128)(2,1)S(1)}, bf16[768,2048]{1,0:T(8,128)(2,1)}, u32[]{:S(2)}) copy-start(bf16[768,2048]{1,0:T(8,128)(2,1)} %all-gather.6.cloned.1.call-done) | copy-start | bytes 9437188
  155.8 25.6 %all-to-all-start.2 = ((bf16[8,96,512]{2,1,0:T(8,128)(2,1)}), bf16[8,96,512]{2,1,0:T(8,128)(2,1)S(1)}, u32[]{:S(2)}, u32[]{:S(2)}) async-start(bf16[8,96,512]{2,1,0:T(8,128)(2,1)} %bitcast.89), calls=%async_computation.3 | async-start | bytes 1572864 | tf_op jit(solution)/shard_map/all_to_all | solution.py:132
  161.3 40.6 %all-gather.8.cloned.1.call-start = ((), (), s32[]{:S(2)}) async-start(), calls=%async_computation.8 | async-start | bytes 1310720 | tf_op jit(solution)/shard_map/all_gather | solution.py:136
  183.3 3.7 %copy-start.2 = (bf16[256,256]{1,0:T(8,128)(2,1)S(1)}, bf16[256,256]{1,0:T(8,128)(2,1)}, u32[]{:S(2)}) copy-start(bf16[256,256]{1,0:T(8,128)(2,1)} %param.15) | copy-start | bytes 393220
  183.3 18.5 %copy-start.9 = (f32[256]{0:T(256)S(1)}, f32[256]{0:T(256)}, u32[]{:S(2)}) copy-start(f32[256]{0:T(256)} %param.17) | copy-start | bytes 3076
  187.0 18.1 %copy-start.7 = (f32[31,256]{1,0:T(8,128)S(1)}, f32[31,256]{1,0:T(8,128)}, u32[]{:S(2)}) copy-start(f32[31,256]{1,0:T(8,128)} %param.16) | copy-start | bytes 95236
  187.0 87.0 %reduce-scatter.5.cloned.1.call-start = ((), (), s32[]{:S(2)}) async-start(), calls=%async_computation.9 | async-start | bytes 2359296 | tf_op jit(solution)/shard_map/reduce_scatter | solution.py:151
  205.1 4.1 %copy-start.11 = (bf16[768,2048]{1,0:T(8,128)(2,1)S(1)}, bf16[768,2048]{1,0:T(8,128)(2,1)}, u32[]{:S(2)}) copy-start(bf16[768,2048]{1,0:T(8,128)(2,1)} %all-gather.4.cloned.1.call-done) | copy-start | bytes 9437188
  205.1 4.1 %copy-start.13 = (f32[768,256]{1,0:T(8,128)S(1)}, f32[768,256]{1,0:T(8,128)}, u32[]{:S(2)}) copy-start(f32[768,256]{1,0:T(8,128)} %fusion.9) | copy-start | bytes 2359300
  205.1 4.1 %copy-start.14 = (f32[768,256]{1,0:T(8,128)S(1)}, f32[768,256]{1,0:T(8,128)}, u32[]{:S(2)}) copy-start(f32[768,256]{1,0:T(8,128)} %fusion.12) | copy-start | bytes 2359300
  209.2 2.1 copy-start.3
  209.2 2.0 copy-start.12
  218.4 8.9 %collective-permute-start = (bf16[15,256]{1,0:T(8,128)(2,1)S(1)}, bf16[15,256]{1,0:T(8,128)(2,1)S(1)}, u32[]{:S(2)}, u32[]{:S(2)}) collective-permute-start(bf16[15,256]{1,0:T(8,128)(2,1)S(1)} %get-tuple-element.18), channel_id=1, source_target_pairs={{0,4},{4,8},{8,12},{12,16},{16,20},{20,24},{24,28},{1,5},{5,9},{9,... | collective-permute-start | bytes 23048 | tf_op jit(solution)/shard_map/ppermute | solution.py:16
  221.9 5.8 %copy-start.5 = (bf16[256,256]{1,0:T(8,128)(2,1)S(1)}, bf16[256,256]{1,0:T(8,128)(2,1)}, u32[]{:S(2)}) copy-start(bf16[256,256]{1,0:T(8,128)(2,1)} %param.14) | copy-start | bytes 393220
  221.9 5.8 %copy-start.6 = (bf16[256,256]{1,0:T(8,128)(2,1)S(1)}, bf16[256,256]{1,0:T(8,128)(2,1)}, u32[]{:S(2)}) copy-start(bf16[256,256]{1,0:T(8,128)(2,1)} %param.13) | copy-start | bytes 393220
  221.9 5.7 %collective-permute-start.1 = (bf16[15,256]{1,0:T(8,128)(2,1)S(1)}, bf16[15,256]{1,0:T(8,128)(2,1)S(1)}, u32[]{:S(2)}, u32[]{:S(2)}) collective-permute-start(bf16[15,256]{1,0:T(8,128)(2,1)S(1)} %get-tuple-element.19), channel_id=1, source_target_pairs={{4,0},{8,4},{12,8},{16,12},{20,16},{24,20},{28,24},{5,1},{9,5},{13... | collective-permute-start | bytes 23048 | tf_op jit(solution)/shard_map/ppermute | solution.py:17
Sparse Core Ops, SparseCore 0:
  44.6 27.5 all-gather.5
  82.7 27.5 all-gather.3
  118.0 37.7 reduce-scatter.2
  187.1 14.6 all-gather.7
  205.8 68.1 reduce-scatter.4
where the time goes:
time: 281 us
  waiting for transfers between devices  133 us (47%)
  blocking collectives  62.7 us (22%)
  matrix products  27.1 us (10%)
  local copies, waits for them, and re-layouts  23.9 us (9%)
  between operations  14.2 us (5%)
  starting transfers between devices  10.8 us (4%)
  other arithmetic  9.13 us (3%)
    reduce_scatter x1, waiting for transfers between devices, per_device(): lax.psum_scatter(lax.dot_general(grad_mix, heads, (((0,), (0,)), ((), ())...  44 us
    reduce_scatter x1, waiting for transfers between devices, per_device(): lax.psum_scatter(partial_value, 'tp', scatter_dimension=2, tiled=True)  37.9 us
    all_to_all x1, blocking collectives, per_device(): lax.all_to_all(in_pad[token_idx], 'sp', split_axis=0, concat_axis=0, tile...  27.3 us
    all_to_all x1, blocking collectives, per_device(): lax.all_to_all(cot_pad[owner_idx], 'sp', split_axis=0, concat_axis=0, til...  23.1 us
    all_gather x1, waiting for transfers between devices, per_device(): lax.all_gather(sent_cot, 'tp', axis=1, tiled=True)  21.8 us
    all_to_all x1, waiting for transfers between devices, per_device(): lax.all_to_all(row_grads, 'sp', split_axis=0, concat_axis=0, tiled=True)  19.8 us
    mul x3, local copies, waits for them, and re-layouts, per_device(): grad_out.astype(jnp.float32)[:, None, :] * route_weights[:, :, None]  10.6 us
    all_gather x1, waiting for transfers between devices, per_device(): grad_mix = lax.all_gather(mix_part, 'tp', axis=1, tiled=True)  8.7 us
  transfers between devices with their start and end apart: 8, of which 6 were waited for; matrix products, arithmetic and copies ran while one was open for 12% of the time, Pallas kernels for 0%

commit v1 on v0

v1 whole, which is shorter than its diff:
```python
import functools
import jax
import jax.numpy as jnp
from jax import lax
from jax.experimental import pallas as pl
from jax.experimental.pallas import tpu as pltpu
from jax.sharding import PartitionSpec as P

MESH = pl.DeviceIdType.MESH
F32 = jnp.float32
BF16 = jnp.bfloat16
HALO = 16
VMEM_LIMIT = 60 * 1024 * 1024


def remote(src, dst, send_sem, recv_sem, device):
    return pltpu.make_async_remote_copy(
        src_ref=src, dst_ref=dst, send_sem=send_sem, recv_sem=recv_sem, device_id=device, device_id_type=MESH
    )


def place(n_sp, n_tp):
    s, t = lax.axis_index("sp"), lax.axis_index("tp")
    core = lax.rem(t, 2)
    mate = t + 1 - 2 * core
    across = lax.rem(t + 2, n_tp)
    return s, t, core, mate, across


def each_peer(s, n_sp, body):
    def step(off, carry):
        body(lax.rem(s + off, n_sp), lax.rem(s + n_sp - off, n_sp))
        return carry

    lax.fori_loop(1, n_sp, step, 0)


def each(n, body):
    def step(i, carry):
        body(i)
        return carry

    lax.fori_loop(0, n, step, 0)


def greet(s, t, n_sp, n_tp):
    barrier = pltpu.get_barrier_semaphore()

    def hello(to, _):
        pl.semaphore_signal(barrier, inc=1, device_id=(to, t), device_id_type=MESH)

    each_peer(s, n_sp, hello)
    for off in range(1, n_tp):
        pl.semaphore_signal(barrier, inc=1, device_id=(s, lax.rem(t + off, n_tp)), device_id_type=MESH)
    pl.semaphore_wait(barrier, n_sp + n_tp - 2)


def dispatch_kernel(n_sp, n_tp, in_ref, cot_ref, st_ref, in_out, cot_out, st_out,
                    i_s, i_r, if_s, if_r, c_s, c_r, cy_s, cy_r, cf_s, cf_r, cg_s, cg_r, st_s, st_r, loc):
    s, t, core, mate, across = place(n_sp, n_tp)
    half, quarter = in_ref.shape[2], cot_ref.shape[2]

    def ci(index):
        return pl.ds(pl.multiple_of(index * half, half), half)

    def cq(index):
        return pl.ds(pl.multiple_of(index * quarter, quarter), quarter)

    greet(s, t, n_sp, n_tp)

    def send_cot(p, dst):
        return remote(cot_ref.at[p], cot_out.at[dst, :, cq(t)], c_s.at[p], c_r.at[dst], (p, t))

    def send_in(p, dst):
        return remote(in_ref.at[p], in_out.at[dst, :, ci(core)], i_s.at[p], i_r.at[dst], (p, t))

    def start(to, _):
        send_cot(to, s).start()
        send_in(to, s).start()

    each_peer(s, n_sp, start)

    def stat(to, row):
        return remote(st_ref, st_out.at[row], st_s.at[to], st_r.at[row], (s, to))

    for off in range(1, n_tp):
        stat(lax.rem(t + off, n_tp), t).start()
    own = [
        pltpu.make_async_copy(in_ref.at[s], in_out.at[s, :, ci(core)], loc.at[0]),
        pltpu.make_async_copy(cot_ref.at[s], cot_out.at[s, :, cq(t)], loc.at[1]),
        pltpu.make_async_copy(st_ref, st_out.at[t], loc.at[2]),
    ]
    for copy in own:
        copy.start()

    def fwd_in(src, p, column):
        return remote(src, in_out.at[p, :, ci(column)], if_s.at[p], if_r.at[p], (s, mate))

    def over_y(src, p, column):
        return remote(src, cot_out.at[p, :, cq(column)], cy_s.at[p], cy_r.at[p], (s, across))

    def fwd_cot(src, p, column):
        return remote(src, cot_out.at[p, :, cq(column)], cf_s.at[p], cf_r.at[p], (s, mate))

    def fwd_far(src, p, column):
        return remote(src, cot_out.at[p, :, cq(column)], cg_s.at[p], cg_r.at[p], (s, mate))

    over_y(cot_ref.at[s], s, t).start()
    fwd_cot(cot_ref.at[s], s, t).start()
    fwd_in(in_ref.at[s], s, core).start()

    def far(p):
        over_y(cot_out.at[p, :, cq(across)], p, across).wait_recv()
        fwd_far(cot_out.at[p, :, cq(across)], p, across).start()

    def forward(_, p):
        send_cot(p, p).wait_recv()
        over_y(cot_out.at[p, :, cq(t)], p, t).start()
        fwd_cot(cot_out.at[p, :, cq(t)], p, t).start()
        send_in(p, p).wait_recv()
        fwd_in(in_out.at[p, :, ci(core)], p, core).start()

    each_peer(s, n_sp, forward)
    far(s)
    each_peer(s, n_sp, lambda _, p: far(p))
    for copy in own:
        copy.wait()
    mate_far = lax.rem(mate + 2, n_tp)

    def finish(p):
        fwd_cot(cot_out.at[p, :, cq(mate)], p, mate).wait_recv()
        fwd_far(cot_out.at[p, :, cq(mate_far)], p, mate_far).wait_recv()
        fwd_in(in_out.at[p, :, ci(1 - core)], p, 1 - core).wait_recv()
        over_y(cot_out.at[p, :, cq(t)], p, t).wait_send()
        fwd_cot(cot_out.at[p, :, cq(t)], p, t).wait_send()
        fwd_far(cot_out.at[p, :, cq(across)], p, across).wait_send()
        fwd_in(in_out.at[p, :, ci(core)], p, core).wait_send()

    each(n_sp, finish)

    def sent(to, _):
        send_cot(to, s).wait_send()
        send_in(to, s).wait_send()

    each_peer(s, n_sp, sent)
    for off in range(1, n_tp):
        other = lax.rem(t + off, n_tp)
        stat(other, other).wait_recv()
        stat(other, t).wait_send()


def dispatch(in_half, cot_quarter, stats, n_sp, n_tp):
    rows, half = in_half.shape[1:]
    vm = pl.BlockSpec(memory_space=pltpu.VMEM)
    per = [pltpu.SemaphoreType.DMA((n_sp,))] * 12
    return pl.pallas_call(
        functools.partial(dispatch_kernel, n_sp, n_tp),
        out_shape=(
            jax.ShapeDtypeStruct((n_sp, rows, 2 * half), BF16),
            jax.ShapeDtypeStruct((n_sp, rows, 2 * half), BF16),
            jax.ShapeDtypeStruct((n_tp,) + stats.shape, F32),
        ),
        in_specs=[vm] * 3,
        out_specs=(vm,) * 3,
        scratch_shapes=per
        + [pltpu.SemaphoreType.DMA((n_tp,)), pltpu.SemaphoreType.DMA((n_tp,)), pltpu.SemaphoreType.DMA((3,))],
        compiler_params=pltpu.CompilerParams(collective_id=0, has_side_effects=True, vmem_limit_bytes=VMEM_LIMIT),
        name="dispatch",
    )(in_half, cot_quarter, stats)


def return_kernel(n_sp, n_tp, chunks, part_ref, pick_ref, go_ref, mix_out, prt, sb, ret, tsend, trecv,
                  m_s, m_r, a_s, a_r, y_s, y_r, g_s, g_r):
    s, t, core, mate, across = place(n_sp, n_tp)
    rows, d_model = part_ref.shape[1:]
    half = d_model // 2
    width = half // chunks
    greet(s, t, n_sp, n_tp)

    def to_mate(p):
        columns = pl.ds(pl.multiple_of((1 - core) * half, half), half)
        return remote(part_ref.at[p, :, columns], prt.at[p], m_s.at[p], m_r.at[p], (s, mate))

    each_peer(s, n_sp, lambda p, _: to_mate(p).start())
    to_mate(s).start()

    def cols(index, k):
        return pl.ds(pl.multiple_of(index * half + k * width, width), width)

    def pair_sum(k, p):
        return (part_ref[p, :, cols(core, k)].astype(F32) + prt[p, :, k * width:(k + 1) * width].astype(F32)).astype(BF16)

    def back(k, p, dst):
        return remote(sb.at[k, p], ret.at[k, dst], a_s.at[k * n_sp + p], a_r.at[k * n_sp + dst], (p, t))

    def cross(k):
        return remote(tsend.at[k], trecv.at[k], y_s.at[k], y_r.at[k], (s, across))

    def share(k, index):
        return remote(mix_out.at[:, cols(index, k)], mix_out.at[:, cols(index, k)], g_s.at[k], g_r.at[k], (s, mate))

    for k in range(chunks):
        def post(p, _, k=k):
            if k == 0:
                to_mate(p).wait_recv()
            sb[k, p] = pair_sum(k, p)
            back(k, p, s).start()

        each_peer(s, n_sp, post)
        if k == 0:
            to_mate(s).wait_recv()
        ret[k, s] = pair_sum(k, s)

    def gather(k):
        each_peer(s, n_sp, lambda _, p: back(k, p, p).wait_recv())
        total = jnp.dot(pick_ref[...], ret[k].reshape(n_sp * rows, width), preferred_element_type=F32)
        tsend[k] = total.astype(BF16)
        cross(k).start()

    def mix(k):
        cross(k).wait_recv()
        mix_out[:, cols(core, k)] = (
            go_ref[:, cols(core, k)].astype(F32) + (tsend[k].astype(F32) + trecv[k].astype(F32))
        ).astype(BF16)
        share(k, core).start()

    for k in range(chunks):
        gather(k)
        if k:
            mix(k - 1)
    mix(chunks - 1)
    for k in range(chunks):
        share(k, 1 - core).wait_recv()
        share(k, core).wait_send()
        cross(k).wait_send()
        each_peer(s, n_sp, lambda p, _, k=k: back(k, p, s).wait_send())
    each(n_sp, lambda p: to_mate(p).wait_send())


def give_back(partial, pick, grad_out, n_sp, n_tp, chunks=2):
    rows, d_model = partial.shape[1:]
    tok = grad_out.shape[0]
    half = d_model // 2
    width = half // chunks
    vm = pl.BlockSpec(memory_space=pltpu.VMEM)
    dma = pltpu.SemaphoreType.DMA
    return pl.pallas_call(
        functools.partial(return_kernel, n_sp, n_tp, chunks),
        out_shape=jax.ShapeDtypeStruct((tok, d_model), BF16),
        in_specs=[vm] * 3,
        out_specs=vm,
        scratch_shapes=[
            pltpu.VMEM((n_sp, rows, half), BF16),
            pltpu.VMEM((chunks, n_sp, rows, width), BF16),
            pltpu.VMEM((chunks, n_sp, rows, width), BF16),
            pltpu.VMEM((chunks, tok, width), BF16),
            pltpu.VMEM((chunks, tok, width), BF16),
            dma((n_sp,)), dma((n_sp,)), dma((chunks * n_sp,)), dma((chunks * n_sp,)),
            dma((chunks,)), dma((chunks,)), dma((chunks,)), dma((chunks,)),
        ],
        compiler_params=pltpu.CompilerParams(collective_id=1, has_side_effects=True, vmem_limit_bytes=VMEM_LIMIT),
        name="give_back",
    )(partial, pick, grad_out)


def tail_kernel(n_sp, n_tp, mix_ref, proj_ref, conv_ref, st_ref, gain_ref, taps_ref, a_ref, b_ref,
                ga_out, gb_out, gop_out, sb, rb, cg, before, after, padded, st_in, st_all,
                p_s, p_r, q_s, q_r, h_s, h_r):
    s, t, core, mate, across = place(n_sp, n_tp)
    tok, width = conv_ref.shape
    share = mix_ref.shape[1] // n_sp
    channels = width * n_tp
    greet(s, t, n_sp, n_tp)
    conv = conv_ref[...].astype(F32)
    stats = st_ref[...]
    mean, rstd = stats[:, 0:1], stats[:, 1:2]
    xhat = (conv - mean) * rstd
    gain = gain_ref[...]
    normed = xhat * gain
    sig = jax.nn.sigmoid(normed)
    heads = (normed * sig).astype(BF16)
    piece = 512
    for i in range(mix_ref.shape[1] // piece):
        sb[i * piece:(i + 1) * piece, :] = lax.dot_general(
            mix_ref[:, i * piece:(i + 1) * piece], heads, (((0,), (0,)), ((), ())), preferred_element_type=F32
        ).astype(BF16)

    def rows_of(p):
        return pl.ds(pl.multiple_of(p * share, 16), share)

    def send(p, dst):
        return remote(sb.at[rows_of(p)], rb.at[dst], p_s.at[p], p_r.at[dst], (p, t))

    each_peer(s, n_sp, lambda p, _: send(p, s).start())

    head = lax.dot_general(mix_ref[...], proj_ref[...], (((1,), (1,)), ((), ())), preferred_element_type=F32)
    grad = head * sig * (1.0 + normed * (1.0 - sig)) * gain
    total = jnp.sum(grad, axis=1, keepdims=True)
    product = jnp.sum(grad * xhat, axis=1, keepdims=True)
    lane = lax.broadcasted_iota(jnp.int32, (tok, 128), 1)
    both = jnp.where(lane == 0, total, jnp.where(lane == 1, product, 0.0))
    st_in[...] = both.T[0:8, :]

    def stat(to, row):
        return remote(st_in, st_all.at[row], q_s.at[to], q_r.at[row], (s, to))

    for off in range(1, n_tp):
        stat(lax.rem(t + off, n_tp), t).start()
    st_all[t] = both.T[0:8, :]
    for off in range(1, n_tp):
        other = lax.rem(t + off, n_tp)
        stat(other, other).wait_recv()
    summed = st_all[0]
    for i in range(1, n_tp):
        summed = summed + st_all[i]
    wide = jnp.concatenate([summed, jnp.zeros((120, tok), F32)], axis=0).T
    cgrad = (
        rstd * (grad - wide[:, 0:1] / channels - xhat * (wide[:, 1:2] / channels))
    ).astype(BF16)
    cg[...] = cgrad

    up = remote(cg.at[tok - HALO:tok], before, h_s.at[0], h_r.at[0], (lax.rem(s + 1, n_sp), t))
    down = remote(cg.at[0:HALO], after, h_s.at[1], h_r.at[1], (lax.rem(s + n_sp - 1, n_sp), t))
    up.start()
    down.start()
    padded[HALO:HALO + tok, :] = cgrad.astype(F32)
    up.wait_recv()
    down.wait_recv()
    padded[0:HALO, :] = jnp.where(s > 0, before[...].astype(F32), 0.0)
    padded[HALO + tok:2 * HALO + tok, :] = jnp.where(s < n_sp - 1, after[...].astype(F32), 0.0)
    taps_n = taps_ref.shape[0]
    reach = (taps_n - 1) // 2
    block = 64
    for r in range(tok // block):
        acc = jnp.zeros((block, width), F32)
        for j in range(taps_n):
            first = r * block + HALO + reach - j
            acc = acc + taps_ref[j:j + 1, :] * padded[first:first + block, :]
        at = slice(r * block, (r + 1) * block)
        sig_b = jax.nn.sigmoid(b_ref[at, :].astype(F32))
        ga_out[at, :] = (acc * sig_b).astype(BF16)
        gb_out[at, :] = (acc * a_ref[at, :].astype(F32) * sig_b * (1.0 - sig_b)).astype(BF16)

    gop_out[...] = sb[rows_of(s), :].astype(F32)

    def add(_, p):
        send(p, p).wait_recv()
        gop_out[...] += rb[p].astype(F32)

    each_peer(s, n_sp, add)
    each_peer(s, n_sp, lambda p, _: send(p, s).wait_send())
    for off in range(1, n_tp):
        stat(lax.rem(t + off, n_tp), t).wait_send()
    up.wait_send()
    down.wait_send()


def tail(mix, proj, conv, stats, gain, taps, glu_a, glu_b, n_sp, n_tp):
    tok, width = conv.shape
    d_model = mix.shape[1]
    vm = pl.BlockSpec(memory_space=pltpu.VMEM)
    dma = pltpu.SemaphoreType.DMA
    return pl.pallas_call(
        functools.partial(tail_kernel, n_sp, n_tp),
        out_shape=(
            jax.ShapeDtypeStruct((tok, width), BF16),
            jax.ShapeDtypeStruct((tok, width), BF16),
            jax.ShapeDtypeStruct((d_model // n_sp, width), F32),
        ),
        in_specs=[vm] * 8,
        out_specs=(vm,) * 3,
        scratch_shapes=[
            pltpu.VMEM((d_model, width), BF16),
            pltpu.VMEM((n_sp, d_model // n_sp, width), BF16),
            pltpu.VMEM((tok, width), BF16),
            pltpu.VMEM((HALO, width), BF16),
            pltpu.VMEM((HALO, width), BF16),
            pltpu.VMEM((tok + 2 * HALO, width), F32),
            pltpu.VMEM((8, tok), F32),
            pltpu.VMEM((n_tp, 8, tok), F32),
            dma((n_sp,)), dma((n_sp,)), dma((n_tp,)), dma((n_tp,)), dma((2,)), dma((2,)),
        ],
        compiler_params=pltpu.CompilerParams(collective_id=2, has_side_effects=True, vmem_limit_bytes=VMEM_LIMIT),
        name="tail",
    )(mix, proj, conv, stats, gain, taps, glu_a, glu_b)


def expert_local(in_rows, cot_rows, w_gate, w_up, w_down):
    gate_pre = jnp.einsum("esd,edf->esf", in_rows, w_gate, preferred_element_type=jnp.float32)
    up_pre = jnp.einsum("esd,edf->esf", in_rows, w_up, preferred_element_type=jnp.float32)
    sig_gate = jax.nn.sigmoid(gate_pre)
    act_gate = gate_pre * sig_gate
    hidden = (act_gate * up_pre).astype(jnp.bfloat16)
    grad_hidden = jnp.einsum("esd,efd->esf", cot_rows, w_down, preferred_element_type=jnp.float32)
    grad_upact = (grad_hidden * act_gate).astype(jnp.bfloat16)
    grad_gateact = (grad_hidden * up_pre * sig_gate * (1.0 + gate_pre * (1.0 - sig_gate))).astype(
        jnp.bfloat16
    )
    return (hidden, grad_upact, grad_gateact)


def weight_grads(in_rows, cot_rows, hidden, grad_upact, grad_gateact):
    grad_down = jnp.einsum(
        "esf,esd->efd", hidden, cot_rows, preferred_element_type=jnp.float32
    ).astype(jnp.bfloat16)
    grad_gate = jnp.einsum(
        "esd,esf->edf", in_rows, grad_gateact, preferred_element_type=jnp.float32
    ).astype(jnp.bfloat16)
    grad_up = jnp.einsum(
        "esd,esf->edf", in_rows, grad_upact, preferred_element_type=jnp.float32
    ).astype(jnp.bfloat16)
    return (grad_gate, grad_up, grad_down)


def per_device(
    glu_a, glu_b, saved_conv, taps, norm_gain_vector, out_proj, moe_in, grad_out, expert_ids, route_weights,
    w_gate, w_up, w_down,
):
    n_sp = lax.axis_size("sp")
    n_tp = lax.axis_size("tp")
    tp_pos = lax.axis_index("tp")
    tok_dev, d_model = grad_out.shape
    top_count = expert_ids.shape[1]
    exp_dev = w_gate.shape[0]
    experts = exp_dev * n_sp
    capacity = max(2, 3 * tok_dev * top_count // (2 * experts))
    capacity = (capacity + 15) // 16 * 16
    channels = saved_conv.shape[1] * n_tp
    half, quarter = d_model // 2, d_model // n_tp
    chosen = expert_ids[:, :, None] == jnp.arange(experts, dtype=jnp.int32)[None, None, :]
    named = jnp.sum(chosen.astype(F32), axis=1)
    places = jnp.arange(tok_dev)
    earlier = (places[:, None] > places[None, :]).astype(BF16)
    before = jnp.dot(earlier, named.astype(BF16), preferred_element_type=F32)
    rank = jnp.sum(jnp.where(chosen, before[:, None, :], 0.0), axis=2).astype(jnp.int32)
    slot_of = expert_ids * capacity + rank
    slots = jnp.arange(experts * capacity, dtype=jnp.int32)
    hits = slot_of[:, :, None] == slots[None, None, :]
    pick = jnp.any(hits, axis=1).astype(BF16)
    row_weight = jnp.sum(jnp.where(hits, route_weights[:, :, None], 0.0), axis=(0, 1))
    in_part = lax.dynamic_slice_in_dim(moe_in, (tp_pos % 2) * half, half, 1)
    cot_part = lax.dynamic_slice_in_dim(grad_out, tp_pos * quarter, quarter, 1)

    def spread(part):
        return lax.dot_general(pick, part, (((0,), (0,)), ((), ())), preferred_element_type=F32)

    in_half = spread(in_part).astype(BF16).reshape(n_sp, exp_dev * capacity, half)
    cot_quarter = (spread(cot_part) * row_weight[:, None]).astype(BF16).reshape(n_sp, exp_dev * capacity, quarter)
    conv = saved_conv.astype(F32)
    sums = jnp.stack([jnp.sum(conv, axis=1), jnp.sum(conv * conv, axis=1)])
    sums = jnp.concatenate([sums, jnp.zeros((6, tok_dev), F32)])
    recv_in, recv_cot, all_sums = dispatch(in_half, cot_quarter, sums, n_sp, n_tp)

    def to_expert(rows):
        return (
            rows.reshape(n_sp, exp_dev, capacity, d_model).swapaxes(0, 1).reshape(exp_dev, n_sp * capacity, d_model)
        )

    in_rows = to_expert(recv_in)
    cot_rows = to_expert(recv_cot)
    hidden, grad_upact, grad_gateact = expert_local(in_rows, cot_rows, w_gate, w_up, w_down)
    partial_value = jnp.einsum("esf,edf->esd", grad_gateact, w_gate, preferred_element_type=F32)
    partial_value = partial_value + jnp.einsum("esf,edf->esd", grad_upact, w_up, preferred_element_type=F32)
    partial_value = (
        partial_value.astype(BF16)
        .reshape(exp_dev, n_sp, capacity, d_model)
        .swapaxes(0, 1)
        .reshape(n_sp, exp_dev * capacity, d_model)
    )
    grad_gate, grad_up, grad_down = weight_grads(in_rows, cot_rows, hidden, grad_upact, grad_gateact)
    grad_mix = give_back(partial_value, pick, grad_out, n_sp, n_tp)
    sum_c, sum_sq = jnp.sum(all_sums, axis=0)[0:2]
    mean = sum_c / channels
    rstd = lax.rsqrt(sum_sq / channels - mean * mean + 1e-05)
    stats = jnp.pad(jnp.stack([mean, rstd], axis=1), ((0, 0), (0, 126)))
    grad_glu_a, grad_glu_b, grad_out_proj = tail(
        grad_mix, out_proj, saved_conv, stats, norm_gain_vector[None, :], taps, glu_a, glu_b, n_sp, n_tp
    )
    return (grad_glu_a, grad_glu_b, grad_out_proj, grad_gate, grad_up, grad_down)


def solution(mesh):
    in_specs = (
        P("sp", "tp"),
        P("sp", "tp"),
        P("sp", "tp"),
        P(None, "tp"),
        P("tp"),
        P("tp", None),
        P("sp", None),
        P("sp", None),
        P("sp", None),
        P("sp", None),
        P("sp", None, "tp"),
        P("sp", None, "tp"),
        P("sp", "tp", None),
    )
    out_specs = (
        P("sp", "tp"),
        P("sp", "tp"),
        P("sp", "tp"),
        P("sp", None, "tp"),
        P("sp", None, "tp"),
        P("sp", "tp", None),
    )
    return jax.shard_map(
        per_device, mesh=mesh, in_specs=in_specs, out_specs=out_specs, check_vma=False
    )
```

time: 281 us -> 189 us (0.67)
  Pallas kernels: 0 us -> 151 us
  waiting for transfers between devices: 133 us -> 0 us
  blocking collectives: 62.7 us -> 0 us
  local copies, waits for them, and re-layouts: 23.9 us -> 6.85 us
  between operations: 14.2 us -> 0.81 us
  starting transfers between devices: 10.8 us -> 0 us
  matrix products: 27.1 us -> 20.4 us
    pallas_call x0 -> x3, Pallas kernels: none -> 151 us  [the longest x1 61.9 us: give_back(): pl.pallas_call(functools.partial(return_kernel, n_sp, n_tp, chunks), out_...]
    reduce_scatter x2 -> x0, waiting for transfers between devices: 81.8 us -> none  [the longest x1 44 us: per_device(): lax.psum_scatter(lax.dot_general(grad_mix, heads, (((0,), (0,)), ((), ())...]
    all_to_all x2 -> x0, blocking collectives: 50.5 us -> none  [the longest x1 27.3 us: per_device(): lax.all_to_all(in_pad[token_idx], 'sp', split_axis=0, concat_axis=0, tile...]
    all_gather x3 -> x0, waiting for transfers between devices: 30.5 us -> none  [the longest x1 21.8 us: per_device(): lax.all_gather(sent_cot, 'tp', axis=1, tiled=True)]
    all_to_all x1 -> x0, waiting for transfers between devices: 19.8 us -> none  [per_device(): lax.all_to_all(row_grads, 'sp', split_axis=0, concat_axis=0, tiled=True)]
    psum x2 -> x0, blocking collectives: 12.2 us -> none  [the longest x1 6.29 us: per_device(): lax.psum((jnp.sum(normalized_gradient, axis=1), jnp.sum(normalized_gradie...]
    mul x5 -> x0, local copies, waits for them, and re-layouts: 10.9 us -> none  [the longest x3 10.6 us: per_device(): grad_out.astype(jnp.float32)[:, None, :] * route_weights[:, :, None]]
    gather x3 -> x0, local copies, waits for them, and re-layouts: 7.33 us -> none  [the longest x1 2.68 us: per_device(): in_pad[token_idx]]
  transfers between devices with their start and end apart: 8 -> 0, of which waited for: 6 -> 0; matrix products, arithmetic and copies ran while one was open for 12% -> 0% of each run, Pallas kernels for 0% -> 0%
where the time goes in v1:
time: 189 us; the launch traced here: 186 us
  Pallas kernels  151 us (80%)
  matrix products  20.4 us (11%)
  local copies, waits for them, and re-layouts  6.85 us (4%)
  other arithmetic  6.65 us (4%)
    pallas_call x1, Pallas kernels, give_back(): pl.pallas_call(functools.partial(return_kernel, n_sp, n_tp, chunks), out_...  61.9 us
    pallas_call x1, Pallas kernels, dispatch(): pl.pallas_call(functools.partial(dispatch_kernel, n_sp, n_tp), out_shape=...  55.3 us
    pallas_call x1, Pallas kernels, tail(): pl.pallas_call(functools.partial(tail_kernel, n_sp, n_tp), out_shape=(jax...  34.1 us
    unnamed x13, local copies, waits for them, and re-layouts  5.97 us
    dot_general x2, matrix products, spread(): lax.dot_general(pick, part, (((0,), (0,)), ((), ())), preferred_element_t...  5.06 us

profile of v1, /device:TPU:0, one launch (start us, length us, event | category | flops | bytes accessed | tf_op | source)
XLA Modules:
  0.0 186.0 jit_solution(13973388312807497527)
XLA Ops:
  0.6 0.0 copy-start
  0.7 0.1 pad.9.clone
  0.7 1.1 convert_reduce_fusion
  1.9 0.7 convert_reduce_fusion.1
  2.6 0.2 fusion.17
  2.7 0.7 select_reduce_fusion.1
  3.4 0.7 convert_add_fusion
  4.1 0.9 select_reduce_fusion
  5.0 0.7 maximum_maximum_fusion.st_ref
  5.7 0.2 fusion.3
  5.9 0.8 convert_element_type.67.pick_ref
  6.7 2.3 %multiply_convert_fusion = bf16[768,512]{1,0:T(8,128)(2,1)} fusion(pred[256,768]{1,0:T(8,128)(4,1)S(1)} %fusion.3, f32[768]{0:T(1024)S(1)} %select_reduce_fusion, bf16[256,2048]{1,0:T(8,128)(2,1)} %go_ref.1, s32[]{:T(128)S(6)} %select_n.24), kind=kOutput, calls=%fused_computation.8 | convolution fusion | flops 202113024 | bytes 1248260 | tf_op jit(solution)/shard_map/dot_general | solution.py:445
  8.9 2.8 %convolution_convert_fusion.3 = bf16[768,1024]{1,0:T(8,128)(2,1)} fusion(pred[256,768]{1,0:T(8,128)(4,1)S(1)} %fusion.3, bf16[256,2048]{1,0:T(8,128)(2,1)} %param.19, s32[]{:T(128)S(6)} %select_n.23), kind=kOutput, calls=%fused_computation.7 | convolution fusion | flops 403439616 | bytes 2293764 | tf_op jit(solution)/shard_map/dot_general | solution.py:445
  11.8 55.3 %dispatch.1 = (bf16[8,96,2048]{2,1,0:T(8,128)(2,1)}, bf16[8,96,2048]{2,1,0:T(8,128)(2,1)}, f32[4,8,256]{2,1,0:T(8,128)}) custom-call(bf16[8,96,1024]{2,1,0:T(8,128)(2,1)} %bitcast.53, bf16[8,96,512]{2,1,0:T(8,128)(2,1)} %bitcast.54, f32[8,256]{1,0:T(8,128)} %maximum_maximum_fusion.st_ref), custom_call_target="tpu_custom_call" | custom-call | tf_op jit(solution)/shard_map/dispatch/pallas_call | solution.py:156
  67.1 0.9 reduce_sum.59
  68.0 0.1 copy.36
  68.1 0.7 pad.4.st_ref
  68.8 3.2 %fusion.6 = f32[768,256]{1,0:T(8,128)S(1)} fusion(bf16[768,2048]{1,0:T(8,128)(2,1)} %bitcast.58, bf16[1,2048,256]{2,1,0:T(8,128)(2,1)S(1)} %copy-done), kind=kOutput, calls=%fused_computation.14 | convolution fusion | flops 805306368 | bytes 4980736 | tf_op jit(solution)/shard_map/esd,edf->esf/dot_general | solution.py:389
  72.0 1.0 fusion.9
  73.0 0.9 copy-done.3
  73.9 0.3 copy-done.4
  74.2 1.2 multiply_convert_fusion.2
  75.4 2.0 %fusion.2 = bf16[1,256,2048]{2,1,0:T(8,128)(2,1)} fusion(bf16[768,2048]{1,0:T(8,128)(2,1)S(1)} %bitcast.63, f32[768,256]{1,0:T(8,128)S(1)} %fusion.9, f32[768,256]{1,0:T(8,128)S(1)} %fusion.6), kind=kOutput, calls=%fused_computation.6 | convolution fusion | flops 807010304 | bytes 5767168 | tf_op jit(solution)/shard_map/esf,esd->efd/dot_general | solution.py:403
  77.4 2.1 %fusion.1 = bf16[1,2048,256]{2,1,0:T(8,128)(2,1)} fusion(bf16[768,2048]{1,0:T(8,128)(2,1)S(1)} %bitcast.60, bf16[768,256]{1,0:T(8,128)(2,1)S(1)} %get-tuple-element.20), kind=kOutput, calls=%fused_computation.5 | convolution fusion | flops 805830656 | bytes 4587520 | tf_op jit(solution)/shard_map/esd,esf->edf/dot_general | solution.py:409
  79.5 2.0 %fusion = bf16[1,2048,256]{2,1,0:T(8,128)(2,1)} fusion(bf16[768,2048]{1,0:T(8,128)(2,1)S(1)} %bitcast.61, bf16[768,256]{1,0:T(8,128)(2,1)S(1)} %get-tuple-element.21), kind=kOutput, calls=%fused_computation.4 | convolution fusion | flops 805830656 | bytes 4587520 | tf_op jit(solution)/shard_map/esd,esf->edf/dot_general | solution.py:406
  81.5 1.0 fusion.4
  82.5 2.7 %add_convert_fusion = bf16[768,2048]{1,0:T(8,128)(2,1)} fusion(f32[768,2048]{1,0:T(8,128)S(1)} %fusion.4, bf16[768,256]{1,0:T(8,128)(2,1)S(1)} %get-tuple-element.20, bf16[1,2048,256]{2,1,0:T(8,128)(2,1)S(1)} %copy-done.1), kind=kOutput, calls=%fused_computation | convolution fusion | flops 808452096 | bytes 10878976 | tf_op jit(solution)/shard_map/esf,edf->esd/dot_general | solution.py:463
  85.2 61.9 %give_back.1.mix_ref = bf16[256,2048]{1,0:T(8,128)(2,1)} custom-call(bf16[8,96,2048]{2,1,0:T(8,128)(2,1)} %bitcast.52, bf16[256,768]{1,0:T(8,128)(2,1)} %convert_element_type.67.pick_ref, bf16[256,2048]{1,0:T(8,128)(2,1)} %go_ref.1), custom_call_target="tpu_custom_call" | custom-call | tf_op jit(solution)/shard_map/give_back/pallas_call | solution.py:247
  147.1 34.1 %tail.1 = (bf16[256,256]{1,0:T(8,128)(2,1)}, bf16[256,256]{1,0:T(8,128)(2,1)}, f32[256,256]{1,0:T(8,128)}) custom-call(bf16[256,2048]{1,0:T(8,128)(2,1)} %give_back.1.mix_ref, bf16[256,2048]{1,0:T(8,128)(2,1)} %proj_ref.1, bf16[256,256]{1,0:T(8,128)(2,1)} %conv_ref.1, f32[256,128]{1,0:T(8,128)} %pad.4.st_ref, f32[1,256]{1,0:T(1,128)} %bitcast.57, ...), custom_call_target="tpu_custom_call" | custom-call | tf_op jit(solution)/shard_map/tail/pallas_call | solution.py:363
  181.2 1.6 copy.40
  182.8 1.6 copy.41
  184.4 1.7 copy.42
  (11 shorter events, 0.0 us)
Async XLA Ops:
  0.6 68.1 %copy-start = (bf16[1,2048,256]{2,1,0:T(8,128)(2,1)S(1)}, bf16[1,2048,256]{2,1,0:T(8,128)(2,1)}, u32[]{:S(2)}) copy-start(bf16[1,2048,256]{2,1,0:T(8,128)(2,1)} %param.23) | copy-start | bytes 3145732
  67.1 4.9 %copy-start.1 = (bf16[1,2048,256]{2,1,0:T(8,128)(2,1)S(1)}, bf16[1,2048,256]{2,1,0:T(8,128)(2,1)}, u32[]{:S(2)}) copy-start(bf16[1,2048,256]{2,1,0:T(8,128)(2,1)} %param.24) | copy-start | bytes 3145732
  68.1 3.9 %copy-start.2 = (bf16[8,96,2048]{2,1,0:T(8,128)(2,1)S(1)}, bf16[8,96,2048]{2,1,0:T(8,128)(2,1)}, u32[]{:S(2)}) copy-start(bf16[8,96,2048]{2,1,0:T(8,128)(2,1)} %get-tuple-element.13) | copy-start | bytes 9437188
  72.0 1.9 %copy-start.3 = (bf16[8,96,2048]{2,1,0:T(8,128)(2,1)S(1)}, bf16[8,96,2048]{2,1,0:T(8,128)(2,1)}, u32[]{:S(2)}) copy-start(bf16[8,96,2048]{2,1,0:T(8,128)(2,1)} %get-tuple-element.12) | copy-start | bytes 9437188
  72.0 2.2 %copy-start.4 = (bf16[1,256,2048]{2,1,0:T(8,128)(2,1)S(1)}, bf16[1,256,2048]{2,1,0:T(8,128)(2,1)}, u32[]{:S(2)}) copy-start(bf16[1,256,2048]{2,1,0:T(8,128)(2,1)} %param.25) | copy-start | bytes 3145732

commit v2 on v1

v2 whole, which is shorter than its diff:
```python
import functools
import jax
import jax.numpy as jnp
from jax import lax
from jax.experimental import pallas as pl
from jax.experimental.pallas import tpu as pltpu
from jax.sharding import PartitionSpec as P

MESH = pl.DeviceIdType.MESH
F32 = jnp.float32
BF16 = jnp.bfloat16
HALO = 16
VMEM_LIMIT = 60 * 1024 * 1024


def remote(src, dst, send_sem, recv_sem, device):
    return pltpu.make_async_remote_copy(
        src_ref=src, dst_ref=dst, send_sem=send_sem, recv_sem=recv_sem, device_id=device, device_id_type=MESH
    )


def place(n_sp, n_tp):
    s, t = lax.axis_index("sp"), lax.axis_index("tp")
    core = lax.rem(t, 2)
    mate = t + 1 - 2 * core
    across = lax.rem(t + 2, n_tp)
    return s, t, core, mate, across


def offset_of(i, n_sp):
    return 1 + lax.rem(i + n_sp // 2 - 1, n_sp - 1)


def each_peer(s, n_sp, body):
    def step(i, carry):
        off = offset_of(i, n_sp)
        body(lax.rem(s + off, n_sp), lax.rem(s + n_sp - off, n_sp))
        return carry

    lax.fori_loop(0, n_sp - 1, step, 0)


def each(n, body):
    def step(i, carry):
        body(i)
        return carry

    lax.fori_loop(0, n, step, 0)


def greet(s, t, n_sp, n_tp):
    barrier = pltpu.get_barrier_semaphore()

    def hello(to, _):
        pl.semaphore_signal(barrier, inc=1, device_id=(to, t), device_id_type=MESH)

    each_peer(s, n_sp, hello)
    for off in range(1, n_tp):
        pl.semaphore_signal(barrier, inc=1, device_id=(s, lax.rem(t + off, n_tp)), device_id_type=MESH)
    pl.semaphore_wait(barrier, n_sp + n_tp - 2)


def dispatch_kernel(n_sp, n_tp, window, rows_ref, st_ref, rows_out, st_out,
                    c_s, c_r, y_s, y_r, f_s, f_r, g_s, g_r, st_s, st_r, loc):
    s, t, core, mate, across = place(n_sp, n_tp)
    quarter = rows_ref.shape[3]
    peers = n_sp - 1
    mate_far = lax.rem(mate + 2, n_tp)

    def cq(index):
        return pl.ds(pl.multiple_of(index * quarter, quarter), quarter)

    def landed(m, p, index):
        return rows_out.at[m, p, :, cq(index)]

    greet(s, t, n_sp, n_tp)

    def send(m, p, dst):
        return remote(rows_ref.at[m, p], landed(m, dst, t), c_s.at[m * n_sp + p], c_r.at[m * n_sp + dst], (p, t))

    def over_y(src, m, p, index):
        return remote(src, landed(m, p, index), y_s.at[m * n_sp + p], y_r.at[m * n_sp + p], (s, across))

    def near(src, m, p, index):
        return remote(src, landed(m, p, index), f_s.at[m * n_sp + p], f_r.at[m * n_sp + p], (s, mate))

    def far(src, m, p, index):
        return remote(src, landed(m, p, index), g_s.at[m * n_sp + p], g_r.at[m * n_sp + p], (s, mate))

    def stat(to, row):
        return remote(st_ref, st_out.at[row], st_s.at[to], st_r.at[row], (s, to))

    def start(j):
        p = lax.rem(s + offset_of(lax.rem(j, peers), n_sp), n_sp)
        send(j // peers, p, s).start()

    each(window, start)
    for off in range(1, n_tp):
        stat(lax.rem(t + off, n_tp), t).start()
    own = [pltpu.make_async_copy(st_ref, st_out.at[t], loc.at[2])]
    for m in range(2):
        own.append(pltpu.make_async_copy(rows_ref.at[m, s], landed(m, s, t), loc.at[m]))
        over_y(rows_ref.at[m, s], m, s, t).start()
        near(rows_ref.at[m, s], m, s, t).start()
    for copy in own:
        copy.start()

    def relay(m, p):
        over_y(landed(m, p, across), m, p, across).wait_recv()
        far(landed(m, p, across), m, p, across).start()

    def forward(j):
        m = j // peers
        p = lax.rem(s + n_sp - offset_of(lax.rem(j, peers), n_sp), n_sp)
        send(m, p, p).wait_recv()
        over_y(landed(m, p, t), m, p, t).start()
        near(landed(m, p, t), m, p, t).start()

    def paced(j):
        start(j + window)
        forward(j)

    each(2 * peers - window, paced)

    def rest(j, carry):
        forward(j)
        return carry

    lax.fori_loop(2 * peers - window, 2 * peers, rest, 0)
    for m in range(2):
        relay(m, s)
    for m in range(2):
        each_peer(s, n_sp, lambda _, p, m=m: relay(m, p))
    for copy in own:
        copy.wait()

    def finish(j):
        m, p = j // n_sp, lax.rem(j, n_sp)
        near(landed(m, p, mate), m, p, mate).wait_recv()
        far(landed(m, p, mate_far), m, p, mate_far).wait_recv()
        over_y(landed(m, p, t), m, p, t).wait_send()
        near(landed(m, p, t), m, p, t).wait_send()
        far(landed(m, p, across), m, p, across).wait_send()

    each(2 * n_sp, finish)
    for m in range(2):
        each_peer(s, n_sp, lambda p, _, m=m: send(m, p, s).wait_send())
    for off in range(1, n_tp):
        other = lax.rem(t + off, n_tp)
        stat(other, other).wait_recv()
        stat(other, t).wait_send()


def dispatch(pair, stats, n_sp, n_tp):
    rows, quarter = pair.shape[2:]
    vm = pl.BlockSpec(memory_space=pltpu.VMEM)
    dma = pltpu.SemaphoreType.DMA
    return pl.pallas_call(
        functools.partial(dispatch_kernel, n_sp, n_tp, min(6, n_sp - 1)),
        out_shape=(
            jax.ShapeDtypeStruct((2, n_sp, rows, n_tp * quarter), BF16),
            jax.ShapeDtypeStruct((n_tp,) + stats.shape, F32),
        ),
        in_specs=[vm] * 2,
        out_specs=(vm,) * 2,
        scratch_shapes=[dma((2 * n_sp,))] * 8 + [dma((n_tp,)), dma((n_tp,)), dma((3,))],
        compiler_params=pltpu.CompilerParams(collective_id=0, has_side_effects=True, vmem_limit_bytes=VMEM_LIMIT),
        name="dispatch",
    )(pair, stats)


def return_kernel(n_sp, n_tp, chunks, window, part_ref, pick_ref, go_ref, mix_out, prt, pair, yr, sb, ret,
                  m_s, m_r, y_s, y_r, a_s, a_r, b_s, b_r, f_s, f_r, g_s, g_r):
    s, t, core, mate, across = place(n_sp, n_tp)
    rows, d_model = part_ref.shape[1:]
    quarter = d_model // n_tp
    width = quarter // chunks
    mate_far = lax.rem(mate + 2, n_tp)
    steps = chunks * n_sp
    greet(s, t, n_sp, n_tp)

    def cq(index, k=0, size=quarter):
        return pl.ds(pl.multiple_of(index * quarter + k * width, width), size)

    def to_mate(p, which, index):
        return remote(
            part_ref.at[p, :, cq(index)], prt.at[which, p], m_s.at[which * n_sp + p], m_r.at[which * n_sp + p], (s, mate)
        )

    def target(i):
        return lax.rem(s + lax.rem(n_sp // 2 + i, n_sp), n_sp)

    def hand(i):
        p = target(i)
        to_mate(p, 1, mate_far).start()
        to_mate(p, 0, mate).start()

    each(n_sp, hand)

    def over_y(k, p):
        return remote(pair.at[k, p], yr.at[k, p], y_s.at[k * n_sp + p], y_r.at[k * n_sp + p], (s, across))

    def back(k, p, dst):
        return remote(sb.at[k, p], ret.at[k, dst], a_s.at[k * n_sp + p], a_r.at[k * n_sp + dst], (p, t))

    def summed(k, p, which, index):
        offset = pl.ds(pl.multiple_of(k * width, width), width)
        return part_ref[p, :, cq(index, k, width)].astype(F32) + prt[which, p, :, offset].astype(F32)

    def post(j):
        k, p = j // n_sp, target(lax.rem(j, n_sp))

        @pl.when(k == 0)
        def _():
            to_mate(p, 1, mate_far).wait_recv()
            to_mate(p, 0, mate).wait_recv()

        pair[k, p] = summed(k, p, 1, across).astype(BF16)
        over_y(k, p).start()

    def settle(j):
        k, p = j // n_sp, target(lax.rem(j, n_sp))
        over_y(k, p).wait_recv()
        sb[k, p] = (summed(k, p, 0, t) + yr[k, p].astype(F32)).astype(BF16)

        @pl.when(p != s)
        def _():
            back(k, p, s).start()

        @pl.when(p == s)
        def _():
            ret[k, s] = sb[k, p]

    each(window, post)

    def paced(j):
        post(j + window)
        settle(j)

    each(steps - window, paced)

    def rest(j, carry):
        settle(j)
        return carry

    lax.fori_loop(steps - window, steps, rest, 0)

    def share(k, index, send_sem, recv_sem, to):
        return remote(
            mix_out.at[:, cq(index, k, width)], mix_out.at[:, cq(index, k, width)], send_sem.at[k], recv_sem.at[k], (s, to)
        )

    for k in range(chunks):
        each_peer(s, n_sp, lambda _, p, k=k: back(k, p, p).wait_recv())
        total = jnp.dot(pick_ref[...], ret[k].reshape(n_sp * rows, width), preferred_element_type=F32)
        mix_out[:, cq(t, k, width)] = (go_ref[:, cq(t, k, width)].astype(F32) + total).astype(BF16)
        share(k, t, b_s, b_r, across).start()
        share(k, t, f_s, f_r, mate).start()
    for k in range(chunks):
        share(k, across, b_s, b_r, across).wait_recv()
        share(k, across, g_s, g_r, mate).start()
    for k in range(chunks):
        share(k, mate, f_s, f_r, mate).wait_recv()
        share(k, mate_far, g_s, g_r, mate).wait_recv()
        share(k, t, b_s, b_r, across).wait_send()
        share(k, t, f_s, f_r, mate).wait_send()
        share(k, across, g_s, g_r, mate).wait_send()
        each_peer(s, n_sp, lambda p, _, k=k: back(k, p, s).wait_send())

    def drained(p):
        to_mate(p, 1, mate_far).wait_send()
        to_mate(p, 0, mate).wait_send()
        for k in range(chunks):
            over_y(k, p).wait_send()

    each(n_sp, drained)


def give_back(partial, pick, grad_out, n_sp, n_tp, chunks=2):
    rows, d_model = partial.shape[1:]
    tok = grad_out.shape[0]
    quarter = d_model // n_tp
    vm = pl.BlockSpec(memory_space=pltpu.VMEM)
    dma = pltpu.SemaphoreType.DMA
    piece = pltpu.VMEM((chunks, n_sp, rows, quarter // chunks), BF16)
    return pl.pallas_call(
        functools.partial(return_kernel, n_sp, n_tp, chunks, min(6, n_sp)),
        out_shape=jax.ShapeDtypeStruct((tok, d_model), BF16),
        in_specs=[vm] * 3,
        out_specs=vm,
        scratch_shapes=[pltpu.VMEM((2, n_sp, rows, quarter), BF16)]
        + [piece] * 4
        + [dma((2 * n_sp,))] * 2
        + [dma((chunks * n_sp,))] * 4
        + [dma((chunks,))] * 6,
        compiler_params=pltpu.CompilerParams(collective_id=1, has_side_effects=True, vmem_limit_bytes=VMEM_LIMIT),
        name="give_back",
    )(partial, pick, grad_out)


def tail_kernel(n_sp, n_tp, mix_ref, proj_ref, conv_ref, st_ref, gain_ref, taps_ref,
                gy_out, rb, sb, nb, sb2, cg, before, after, padded, st_in, st_all,
                n_s, n_r, p_s, p_r, q_s, q_r, h_s, h_r):
    s, t, core, mate, across = place(n_sp, n_tp)
    tok, width = conv_ref.shape
    share = mix_ref.shape[1] // n_sp
    channels = width * n_tp
    greet(s, t, n_sp, n_tp)
    conv = conv_ref[...].astype(F32)
    stats = st_ref[...]
    mean, rstd = stats[:, 0:1], stats[:, 1:2]
    xhat = (conv - mean) * rstd
    gain = gain_ref[...]
    normed = xhat * gain
    sig = jax.nn.sigmoid(normed)
    heads = (normed * sig).astype(BF16)
    piece = 512
    for i in range(mix_ref.shape[1] // piece):
        sb[i * piece:(i + 1) * piece, :] = lax.dot_general(
            mix_ref[:, i * piece:(i + 1) * piece], heads, (((0,), (0,)), ((), ())), preferred_element_type=F32
        ).astype(BF16)

    def rows_of(p):
        return pl.ds(pl.multiple_of(p * share, 16), share)

    groups = n_sp // 2
    side, group = lax.rem(s, 2), s // 2
    partner = s + 1 - 2 * side

    def pool(g, index):
        return remote(sb.at[rows_of(2 * g + index)], nb.at[g], n_s.at[g], n_r.at[g], (partner, t))

    def send(g, dst):
        return remote(sb2.at[g], rb.at[dst], p_s.at[g], p_r.at[dst], (2 * g + side, t))

    def target(i):
        return lax.rem(group + lax.rem(groups // 2 + i, groups), groups)

    each(groups, lambda i: pool(target(i), 1 - side).start())

    head = lax.dot_general(mix_ref[...], proj_ref[...], (((1,), (1,)), ((), ())), preferred_element_type=F32)
    grad = head * sig * (1.0 + normed * (1.0 - sig)) * gain
    total = jnp.sum(grad, axis=1, keepdims=True)
    product = jnp.sum(grad * xhat, axis=1, keepdims=True)
    lane = lax.broadcasted_iota(jnp.int32, (tok, 128), 1)
    both = jnp.where(lane == 0, total, jnp.where(lane == 1, product, 0.0))
    st_in[...] = both.T[0:8, :]

    def stat(to, row):
        return remote(st_in, st_all.at[row], q_s.at[to], q_r.at[row], (s, to))

    for off in range(1, n_tp):
        stat(lax.rem(t + off, n_tp), t).start()
    st_all[t] = both.T[0:8, :]
    for off in range(1, n_tp):
        other = lax.rem(t + off, n_tp)
        stat(other, other).wait_recv()
    summed = st_all[0]
    for i in range(1, n_tp):
        summed = summed + st_all[i]
    wide = jnp.concatenate([summed, jnp.zeros((120, tok), F32)], axis=0).T
    cgrad = (
        rstd * (grad - wide[:, 0:1] / channels - xhat * (wide[:, 1:2] / channels))
    ).astype(BF16)
    cg[...] = cgrad

    up = remote(cg.at[tok - HALO:tok], before, h_s.at[0], h_r.at[0], (lax.rem(s + 1, n_sp), t))
    down = remote(cg.at[0:HALO], after, h_s.at[1], h_r.at[1], (lax.rem(s + n_sp - 1, n_sp), t))
    up.start()
    down.start()
    padded[HALO:HALO + tok, :] = cgrad.astype(F32)
    def pooled(i):
        g = target(i)
        pool(g, side).wait_recv()
        sb2[g] = (sb[rows_of(2 * g + side), :].astype(F32) + nb[g].astype(F32)).astype(BF16)

        @pl.when(g != group)
        def _():
            send(g, group).start()

        @pl.when(g == group)
        def _():
            rb[group] = sb2[g]

    each(groups, pooled)
    up.wait_recv()
    down.wait_recv()
    padded[0:HALO, :] = jnp.where(s > 0, before[...].astype(F32), 0.0)
    padded[HALO + tok:2 * HALO + tok, :] = jnp.where(s < n_sp - 1, after[...].astype(F32), 0.0)
    taps_n = taps_ref.shape[0]
    reach = (taps_n - 1) // 2
    block = 64
    for r in range(tok // block):
        acc = jnp.zeros((block, width), F32)
        for j in range(taps_n):
            first = r * block + HALO + reach - j
            acc = acc + taps_ref[j:j + 1, :] * padded[first:first + block, :]
        at = slice(r * block, (r + 1) * block)
        gy_out[at, :] = acc

    def others(body):
        each(groups, lambda g: pl.when(g != group)(lambda: body(g)))

    others(lambda g: send(g, g).wait_recv())
    others(lambda g: send(g, group).wait_send())
    each(groups, lambda g: pool(g, 1 - side).wait_send())
    for off in range(1, n_tp):
        stat(lax.rem(t + off, n_tp), t).wait_send()
    up.wait_send()
    down.wait_send()


def tail(mix, proj, conv, stats, gain, taps, n_sp, n_tp):
    tok, width = conv.shape
    d_model = mix.shape[1]
    vm = pl.BlockSpec(memory_space=pltpu.VMEM)
    dma = pltpu.SemaphoreType.DMA
    return pl.pallas_call(
        functools.partial(tail_kernel, n_sp, n_tp),
        out_shape=(
            jax.ShapeDtypeStruct((tok, width), F32),
            jax.ShapeDtypeStruct((n_sp // 2, d_model // n_sp, width), BF16),
        ),
        in_specs=[vm] * 6,
        out_specs=(vm,) * 2,
        scratch_shapes=[
            pltpu.VMEM((d_model, width), BF16),
            pltpu.VMEM((n_sp // 2, d_model // n_sp, width), BF16),
            pltpu.VMEM((n_sp // 2, d_model // n_sp, width), BF16),
            pltpu.VMEM((tok, width), BF16),
            pltpu.VMEM((HALO, width), BF16),
            pltpu.VMEM((HALO, width), BF16),
            pltpu.VMEM((tok + 2 * HALO, width), F32),
            pltpu.VMEM((8, tok), F32),
            pltpu.VMEM((n_tp, 8, tok), F32),
            dma((n_sp // 2,)), dma((n_sp // 2,)), dma((n_sp // 2,)), dma((n_sp // 2,)),
            dma((n_tp,)), dma((n_tp,)), dma((2,)), dma((2,)),
        ],
        compiler_params=pltpu.CompilerParams(collective_id=2, has_side_effects=True, vmem_limit_bytes=VMEM_LIMIT),
        name="tail",
    )(mix, proj, conv, stats, gain, taps)


def expert_local(in_rows, cot_rows, w_gate, w_up, w_down):
    gate_pre = jnp.einsum("esd,edf->esf", in_rows, w_gate, preferred_element_type=jnp.float32)
    up_pre = jnp.einsum("esd,edf->esf", in_rows, w_up, preferred_element_type=jnp.float32)
    sig_gate = jax.nn.sigmoid(gate_pre)
    act_gate = gate_pre * sig_gate
    hidden = (act_gate * up_pre).astype(jnp.bfloat16)
    grad_hidden = jnp.einsum("esd,efd->esf", cot_rows, w_down, preferred_element_type=jnp.float32)
    grad_upact = (grad_hidden * act_gate).astype(jnp.bfloat16)
    grad_gateact = (grad_hidden * up_pre * sig_gate * (1.0 + gate_pre * (1.0 - sig_gate))).astype(
        jnp.bfloat16
    )
    return (hidden, grad_upact, grad_gateact)


def weight_grads(in_rows, cot_rows, hidden, grad_upact, grad_gateact):
    grad_down = jnp.einsum(
        "esf,esd->efd", hidden, cot_rows, preferred_element_type=jnp.float32
    ).astype(jnp.bfloat16)
    grad_gate = jnp.einsum(
        "esd,esf->edf", in_rows, grad_gateact, preferred_element_type=jnp.float32
    ).astype(jnp.bfloat16)
    grad_up = jnp.einsum(
        "esd,esf->edf", in_rows, grad_upact, preferred_element_type=jnp.float32
    ).astype(jnp.bfloat16)
    return (grad_gate, grad_up, grad_down)


def per_device(
    glu_a, glu_b, saved_conv, taps, norm_gain_vector, out_proj, moe_in, grad_out, expert_ids, route_weights,
    w_gate, w_up, w_down,
):
    n_sp = lax.axis_size("sp")
    n_tp = lax.axis_size("tp")
    tp_pos = lax.axis_index("tp")
    tok_dev, d_model = grad_out.shape
    top_count = expert_ids.shape[1]
    exp_dev = w_gate.shape[0]
    experts = exp_dev * n_sp
    capacity = max(2, 3 * tok_dev * top_count // (2 * experts))
    capacity = (capacity + 15) // 16 * 16
    channels = saved_conv.shape[1] * n_tp
    quarter = d_model // n_tp
    chosen = expert_ids[:, :, None] == jnp.arange(experts, dtype=jnp.int32)[None, None, :]
    named = jnp.sum(chosen.astype(F32), axis=1)
    places = jnp.arange(tok_dev)
    earlier = (places[:, None] > places[None, :]).astype(BF16)
    before = jnp.dot(earlier, named.astype(BF16), preferred_element_type=F32)
    rank = jnp.sum(jnp.where(chosen, before[:, None, :], 0.0), axis=2).astype(jnp.int32)
    slot_of = expert_ids * capacity + rank
    slots = jnp.arange(experts * capacity, dtype=jnp.int32)
    hits = slot_of[:, :, None] == slots[None, None, :]
    pick = jnp.any(hits, axis=1).astype(BF16)
    row_weight = jnp.sum(jnp.where(hits, route_weights[:, :, None], 0.0), axis=(0, 1))
    in_part = lax.dynamic_slice_in_dim(moe_in, tp_pos * quarter, quarter, 1)
    cot_part = lax.dynamic_slice_in_dim(grad_out, tp_pos * quarter, quarter, 1)

    def spread(part):
        return lax.dot_general(pick, part, (((0,), (0,)), ((), ())), preferred_element_type=F32)

    pair = jnp.stack([spread(in_part).astype(BF16), (spread(cot_part) * row_weight[:, None]).astype(BF16)])
    pair = pair.reshape(2, n_sp, exp_dev * capacity, quarter)
    conv = saved_conv.astype(F32)
    sums = jnp.stack([jnp.sum(conv, axis=1), jnp.sum(conv * conv, axis=1)])
    sums = jnp.concatenate([sums, jnp.zeros((6, tok_dev), F32)])
    received, all_sums = dispatch(pair, sums, n_sp, n_tp)

    def to_expert(rows):
        return (
            rows.reshape(n_sp, exp_dev, capacity, d_model).swapaxes(0, 1).reshape(exp_dev, n_sp * capacity, d_model)
        )

    in_rows = to_expert(received[0])
    cot_rows = to_expert(received[1])
    hidden, grad_upact, grad_gateact = expert_local(in_rows, cot_rows, w_gate, w_up, w_down)
    partial_value = jnp.einsum("esf,edf->esd", grad_gateact, w_gate, preferred_element_type=F32)
    partial_value = partial_value + jnp.einsum("esf,edf->esd", grad_upact, w_up, preferred_element_type=F32)
    partial_value = (
        partial_value.astype(BF16)
        .reshape(exp_dev, n_sp, capacity, d_model)
        .swapaxes(0, 1)
        .reshape(n_sp, exp_dev * capacity, d_model)
    )
    grad_gate, grad_up, grad_down = weight_grads(in_rows, cot_rows, hidden, grad_upact, grad_gateact)
    grad_mix = give_back(partial_value, pick, grad_out, n_sp, n_tp)
    sum_c, sum_sq = jnp.sum(all_sums, axis=0)[0:2]
    mean = sum_c / channels
    rstd = lax.rsqrt(sum_sq / channels - mean * mean + 1e-05)
    stats = jnp.pad(jnp.stack([mean, rstd], axis=1), ((0, 0), (0, 126)))
    grad_y, shares = tail(grad_mix, out_proj, saved_conv, stats, norm_gain_vector[None, :], taps, n_sp, n_tp)
    grad_out_proj = jnp.sum(shares.astype(F32), axis=0)
    sig_b = jax.nn.sigmoid(glu_b.astype(F32))
    grad_glu_a = (grad_y * sig_b).astype(BF16)
    grad_glu_b = (grad_y * glu_a.astype(F32) * sig_b * (1.0 - sig_b)).astype(BF16)
    return (grad_glu_a, grad_glu_b, grad_out_proj, grad_gate, grad_up, grad_down)


def solution(mesh):
    in_specs = (
        P("sp", "tp"),
        P("sp", "tp"),
        P("sp", "tp"),
        P(None, "tp"),
        P("tp"),
        P("tp", None),
        P("sp", None),
        P("sp", None),
        P("sp", None),
        P("sp", None),
        P("sp", None, "tp"),
        P("sp", None, "tp"),
        P("sp", "tp", None),
    )
    out_specs = (
        P("sp", "tp"),
        P("sp", "tp"),
        P("sp", "tp"),
        P("sp", None, "tp"),
        P("sp", None, "tp"),
        P("sp", "tp", None),
    )
    return jax.shard_map(
        per_device, mesh=mesh, in_specs=in_specs, out_specs=out_specs, check_vma=False
    )
```

time: 189 us -> 155 us (0.82); the launches traced: 186 us -> 155 us
  Pallas kernels: 151 us -> 124 us
  matrix products: 20.4 us -> 15.9 us
  other arithmetic: 6.65 us -> 9.84 us
  local copies, waits for them, and re-layouts: 6.85 us -> 4.56 us
    pallas_call x2, Pallas kernels: 117 us -> 99.1 us  [the longest x1 56 us: dispatch(): pl.pallas_call(functools.partial(dispatch_kernel, n_sp, n_tp, min(6, n_sp...]
    pallas_call x1, Pallas kernels: 34.1 us -> 24.4 us  [tail(): pl.pallas_call(functools.partial(tail_kernel, n_sp, n_tp), out_shape=(jax...]
    unnamed x13 -> x14, local copies, waits for them, and re-layouts: 5.97 us -> 0.25 us
    slice x0 -> x1, local copies, waits for them, and re-layouts: none -> 3.43 us  [per_device(): cot_rows = to_expert(received[1])]
    dot_general x2, matrix products: 5.06 us -> 2.75 us  [spread(): lax.dot_general(pick, part, (((0,), (0,)), ((), ())), preferred_element_t...]
    dot_general x1, matrix products: 3.19 us -> 0.98 us  [expert_local(): jnp.einsum('esd,edf->esf', in_rows, w_gate, preferred_element_type=jnp.fl...]
where the time goes in v2:
time: 155 us
  Pallas kernels  124 us (80%)
  matrix products  15.9 us (10%)
  other arithmetic  9.84 us (6%)
  local copies, waits for them, and re-layouts  4.56 us (3%)
    pallas_call x1, Pallas kernels, dispatch(): pl.pallas_call(functools.partial(dispatch_kernel, n_sp, n_tp, min(6, n_sp...  56 us
    pallas_call x1, Pallas kernels, give_back(): pl.pallas_call(functools.partial(return_kernel, n_sp, n_tp, chunks, min(6...  43.1 us
    pallas_call x1, Pallas kernels, tail(): pl.pallas_call(functools.partial(tail_kernel, n_sp, n_tp), out_shape=(jax...  24.4 us
    slice x1, local copies, waits for them, and re-layouts, per_device(): cot_rows = to_expert(received[1])  3.43 us

profile of v2, /device:TPU:0, one launch (start us, length us, event | category | flops | bytes accessed | tf_op | source)
XLA Modules:
  0.0 154.7 jit_solution(6190146737335437727)
XLA Ops:
  0.6 0.0 copy-start
  0.6 0.0 copy-start.2
  0.7 0.8 convert_reduce_fusion.2
  1.5 0.2 fusion.17
  1.6 0.7 select_reduce_fusion.1
  2.4 0.7 convert_add_fusion
  3.0 0.2 fusion.3
  3.2 0.9 select_reduce_fusion
  4.2 1.4 multiply_convert_fusion
  5.5 1.4 convolution_convert_fusion.3
  6.9 1.3 pad_maximum_fusion.rows_ref
  8.2 0.1 convert_reduce_fusion.1
  8.4 0.1 pad.9.clone
  8.5 0.7 maximum_maximum_fusion.st_ref
  9.1 56.0 %dispatch.1 = (bf16[2,8,96,2048]{3,2,1,0:T(8,128)(2,1)}, f32[4,8,256]{2,1,0:T(8,128)}) custom-call(bf16[2,8,96,512]{3,2,1,0:T(8,128)(2,1)} %pad_maximum_fusion.rows_ref, f32[8,256]{1,0:T(8,128)} %maximum_maximum_fusion.st_ref), custom_call_target="tpu_custom_call" | custom-call | tf_op jit(solution)/shard_map/dispatch/pallas_call | solution.py:158
  65.1 3.4 %fusion.26 = (bf16[1,8,96,2048]{3,2,1,0:T(8,128)(2,1)S(1)}, bf16[1,8,96,2048]{3,2,1,0:T(8,128)(2,1)S(1)}) fusion(bf16[2,8,96,2048]{3,2,1,0:T(8,128)(2,1)} %get-tuple-element.10), kind=kLoop, calls=%fused_computation.54 | loop fusion | bytes 12582912 | tf_op jit(solution)/shard_map/slice | solution.py:516
  68.6 1.0 fusion.6
  69.6 0.2 copy-done.1
  69.8 1.0 fusion.9
  70.8 2.1 %fusion.2 = bf16[1,256,2048]{2,1,0:T(8,128)(2,1)} fusion(bf16[768,2048]{1,0:T(8,128)(2,1)S(1)} %bitcast.58, f32[768,256]{1,0:T(8,128)S(1)} %fusion.9, f32[768,256]{1,0:T(8,128)S(1)} %fusion.6), kind=kOutput, calls=%fused_computation.6 | convolution fusion | flops 807010304 | bytes 5767168 | tf_op jit(solution)/shard_map/esf,esd->efd/dot_general | solution.py:459
  72.9 1.3 multiply_convert_fusion.2
  74.1 2.0 %fusion.1 = bf16[1,2048,256]{2,1,0:T(8,128)(2,1)} fusion(bf16[768,2048]{1,0:T(8,128)(2,1)S(1)} %bitcast.56, bf16[768,256]{1,0:T(8,128)(2,1)S(1)} %get-tuple-element.18), kind=kOutput, calls=%fused_computation.5 | convolution fusion | flops 805830656 | bytes 4587520 | tf_op jit(solution)/shard_map/esd,esf->edf/dot_general | solution.py:465
  76.1 2.0 %fusion = bf16[1,2048,256]{2,1,0:T(8,128)(2,1)} fusion(bf16[768,2048]{1,0:T(8,128)(2,1)S(1)} %bitcast.57, bf16[768,256]{1,0:T(8,128)(2,1)S(1)} %get-tuple-element.19), kind=kOutput, calls=%fused_computation.4 | convolution fusion | flops 805830656 | bytes 4587520 | tf_op jit(solution)/shard_map/esd,esf->edf/dot_general | solution.py:462
  78.2 1.0 fusion.4
  79.2 2.7 %add_convert_fusion = bf16[768,2048]{1,0:T(8,128)(2,1)} fusion(f32[768,2048]{1,0:T(8,128)S(1)} %fusion.4, bf16[768,256]{1,0:T(8,128)(2,1)S(1)} %get-tuple-element.18, bf16[1,2048,256]{2,1,0:T(8,128)(2,1)S(1)} %copy-done.1), kind=kOutput, calls=%fused_computation | convolution fusion | flops 808452096 | bytes 10878976 | tf_op jit(solution)/shard_map/esf,edf->esd/dot_general | solution.py:519
  81.9 0.8 convert_element_type.82.pick_ref
  82.7 43.1 %give_back.1.mix_ref = bf16[256,2048]{1,0:T(8,128)(2,1)} custom-call(bf16[8,96,2048]{2,1,0:T(8,128)(2,1)} %bitcast.52, bf16[256,768]{1,0:T(8,128)(2,1)} %convert_element_type.82.pick_ref, bf16[256,2048]{1,0:T(8,128)(2,1)} %go_ref.1), custom_call_target="tpu_custom_call" | custom-call | tf_op jit(solution)/shard_map/give_back/pallas_call | solution.py:286
  125.9 0.1 copy.36
  126.0 0.7 pad.4.st_ref
  126.7 24.4 %tail.1 = (f32[256,256]{1,0:T(8,128)}, bf16[4,256,256]{2,1,0:T(8,128)(2,1)}) custom-call(bf16[256,2048]{1,0:T(8,128)(2,1)} %give_back.1.mix_ref, bf16[256,2048]{1,0:T(8,128)(2,1)} %proj_ref.1, bf16[256,256]{1,0:T(8,128)(2,1)} %conv_ref.1, f32[256,128]{1,0:T(8,128)} %pad.4.st_ref, f32[1,256]{1,0:T(1,128)} %bitcast.63, f32[31,256]{1,0:T(8,128)} %taps_ref.1), custom_call_target="tpu_custom_call" | custom-call | tf_op jit(solution)/shard_map/tail/pallas_call | solution.py:418
  151.2 1.8 %multiply_convert_fusion.5 = (bf16[256,256]{1,0:T(8,128)(2,1)}, bf16[256,256]{1,0:T(8,128)(2,1)}) fusion(f32[256,256]{1,0:T(8,128)} %get-tuple-element.12, bf16[256,256]{1,0:T(8,128)(2,1)S(1)} %copy-done.3, bf16[256,256]{1,0:T(8,128)(2,1)S(1)} %copy-done.4), kind=kLoop, calls=%fused_computation.31 | loop fusion | flops 786432 | bytes 786432 | tf_op jit(solution)/shard_map/convert_element_type | solution.py:536
  152.9 1.8 %convert_reduce_fusion = f32[256,256]{1,0:T(8,128)} fusion(bf16[4,256,256]{2,1,0:T(8,128)(2,1)} %get-tuple-element.13), kind=kLoop, calls=%fused_computation.22 | loop fusion | flops 458752 | bytes 786432 | tf_op jit(solution)/shard_map/reduce_sum | solution.py:533
  (16 shorter events, 0.1 us)
Async XLA Ops:
  0.6 67.9 %copy-start = (bf16[1,2048,256]{2,1,0:T(8,128)(2,1)S(1)}, bf16[1,2048,256]{2,1,0:T(8,128)(2,1)}, u32[]{:S(2)}) copy-start(bf16[1,2048,256]{2,1,0:T(8,128)(2,1)} %param.23) | copy-start | bytes 3145732
  0.6 7.6 %copy-start.2 = (bf16[256,256]{1,0:T(8,128)(2,1)S(1)}, bf16[256,256]{1,0:T(8,128)(2,1)}, u32[]{:S(2)}) copy-start(bf16[256,256]{1,0:T(8,128)(2,1)} %conv_ref.1) | copy-start | bytes 393220
  68.6 1.2 copy-start.1
  70.8 2.1 %copy-start.6 = (bf16[1,256,2048]{2,1,0:T(8,128)(2,1)S(1)}, bf16[1,256,2048]{2,1,0:T(8,128)(2,1)}, u32[]{:S(2)}) copy-start(bf16[1,256,2048]{2,1,0:T(8,128)(2,1)} %param.25) | copy-start | bytes 3145732
  81.9 43.9 %copy-start.5 = (f32[4,8,256]{2,1,0:T(8,128)S(1)}, f32[4,8,256]{2,1,0:T(8,128)}, u32[]{:S(2)}) copy-start(f32[4,8,256]{2,1,0:T(8,128)} %get-tuple-element.11) | copy-start | bytes 98308
  82.6 68.5 %copy-start.3 = (bf16[256,256]{1,0:T(8,128)(2,1)S(1)}, bf16[256,256]{1,0:T(8,128)(2,1)}, u32[]{:S(2)}) copy-start(bf16[256,256]{1,0:T(8,128)(2,1)} %param.13) | copy-start | bytes 393220
  82.7 68.5 %copy-start.4 = (bf16[256,256]{1,0:T(8,128)(2,1)S(1)}, bf16[256,256]{1,0:T(8,128)(2,1)}, u32[]{:S(2)}) copy-start(bf16[256,256]{1,0:T(8,128)(2,1)} %param.14) | copy-start | bytes 393220
